TPU v7x, 128 devices: a whole 4x4x4 slice. The times are simulated.
128 devices in a mesh: ep: 16 (over z, x), tp: 8 (over y, core).
Axes of the slice: x: 4, y: 4, z: 4, core: 2. Of those that a mesh axis runs over, the one named last changes fastest.
Arguments:
- query_latent: bfloat16 [16384, 768], P(('ep', 'tp')), may hold values from -6 to 6
- kv_latent: bfloat16 [16384, 512], P(('ep', 'tp')), may hold values from -6 to 6
- rope_key: bfloat16 [16384, 64], P(('ep', 'tp')), may hold values from -6 to 6
- query_gain: float32 [768], replicated, may hold values from 0.1 to 12
- kv_gain: float32 [512], replicated, may hold values from 0.1 to 12
- query_nope_w: bfloat16 [768, 1024], P(None, 'tp'), may hold values from -0.21875 to 0.21875
- query_rope_w: bfloat16 [768, 512], P(None, 'tp'), may hold values from -0.21875 to 0.21875
- key_up_w: bfloat16 [512, 1024], P(None, 'tp'), may hold values from -0.25 to 0.25
- value_up_w: bfloat16 [512, 1024], P(None, 'tp'), may hold values from -0.25 to 0.25
- output_w: bfloat16 [1024, 2048], P('tp'), may hold values from -0.1875 to 0.1875
- expert_in: bfloat16 [16384, 2048], P(('ep', 'tp')), may hold values from -6 to 6
- moe_gain: float32 [2048], replicated, may hold values from 0.1 to 12
- routes: int32 [16384, 2], P(('ep', 'tp')), may hold values from 0 to 31, all different within a row; in each aligned block of 128 rows (0 to 127, 128 to 255, ...) at most 10 rows name the same one
- route_weight: float32 [16384, 2], P(('ep', 'tp')), may hold values from 0.1 to 1
- gate_w: bfloat16 [32, 2048, 2048], P('ep', None, 'tp'), may hold values from -0.125 to 0.125
- up_w: bfloat16 [32, 2048, 2048], P('ep', None, 'tp'), may hold values from -0.125 to 0.125
- down_w: bfloat16 [32, 2048, 2048], P('ep', 'tp'), may hold values from -0.125 to 0.125
Outputs:
- mixer_out: bfloat16 [16384, 2048], P(('ep', 'tp'))
- expert_out: bfloat16 [16384, 2048], P(('ep', 'tp'))
Inputs may be any that keep to these rules, and one draw needn't show every extreme that they name: `routes`: each row names 2 different experts; in the rows of one device no expert is named more than 10 times.
All inputs are finite; a program needn't handle non-finite values.
Results may differ from a plain program's by a relative error of at most 0.015.
The roundings to bfloat16 on the way count: a program that leaves them out, or rounds other values in their place, can miss the bound.
Values may be sent and summed in bfloat16 or wider, within the bound.
A program may use at most 128 MiB of HBM per device.

v0:
```python
import functools
import math

import jax
import jax.numpy as jnp
from jax import lax
from jax.experimental import pallas as pl
from jax.experimental.pallas import tpu as pltpu
from jax.sharding import PartitionSpec as P

BF = jnp.bfloat16
F32 = jnp.float32
NOPE, ROPE, VDIM = 128, 64, 128
QLAT, KVLAT, D = 768, 512, 2048
HID = 256
TOK = 128
GROUP = 1024
HALF = 512
LAT = QLAT + KVLAT + 128
KVR = HALF + HALF + HALF // 2
KVH = KVR // 2
QT = 256
THETA = 10000.0
MESH = pl.DeviceIdType.MESH
SCALE2 = math.log2(math.e) / math.sqrt(NOPE + ROPE)
VM = pltpu.VMEM


def dot(a, b):
    return jnp.dot(a, b, preferred_element_type=F32)


def kernel(
    ql_ref, kl_ref, kr_ref, qg_ref, kg_ref, ct_ref, st_ref, wq_ref, wr_ref, wk_ref, wv_ref,
    xin_ref, mg_ref, routes_ref, rw_ref, ow_hbm, gw_hbm, uw_hbm, dw_hbm,
    omix_ref, oexp_ref,
    lat, kv, qa, qb, m_s, l_s, acc, att_loc, att_snd, att_rcv,
    ow, gw, uw, dw,
    out, xb, bb, back, pp, ra, rb, rc, sb,
    pm, ma, mb, mc, ms, sid_s, nrm,
    loc_sem, m1_s, m1_r, w_s, w_r, a1_s, a1_r, d1_s, d1_r,
    p1_s, p1_r, p2_s, p2_r, x1_s, x1_r, x2_s, x2_r,
    r_s, r_r, t_s, t_r, at_s, at_r, m5_s, m5_r,
):
    ep = lax.axis_index("ep")
    tp = lax.axis_index("tp")
    y, core = tp // 2, tp % 2
    z, x = ep // 4, ep % 4
    mate = {"ep": ep, "tp": y * 2 + 1 - core}

    def wrap(a):
        return (a + 4) % 4

    def at_y(dy):
        return {"ep": ep, "tp": wrap(y + dy) * 2 + core}

    def at_ep(e):
        return {"ep": e, "tp": tp}

    def remote(src, dst, ssem, rsem, dev):
        return pltpu.make_async_remote_copy(
            src_ref=src, dst_ref=dst, send_sem=ssem, recv_sem=rsem, device_id=dev, device_id_type=MESH
        )

    barrier = pltpu.get_barrier_semaphore()
    for dy in (1, 2, 3):
        pl.semaphore_signal(barrier, inc=1, device_id=at_y(dy), device_id_type=MESH)
    pl.semaphore_signal(barrier, inc=1, device_id=mate, device_id_type=MESH)

    def greet(k, c):
        pl.semaphore_signal(barrier, inc=1, device_id=at_ep((ep + k) % 16), device_id_type=MESH)
        return c

    lax.fori_loop(1, 16, greet, 0)

    locals_ = [
        pltpu.make_async_copy(gw_hbm, gw.at[0], loc_sem.at[0]),
        pltpu.make_async_copy(uw_hbm, uw.at[0], loc_sem.at[1]),
        pltpu.make_async_copy(dw_hbm, dw.at[0], loc_sem.at[2]),
        pltpu.make_async_copy(ow_hbm, ow.at[0], loc_sem.at[3]),
    ]
    for c in locals_:
        c.start()

    f = xin_ref[...].astype(F32)
    cen = f - jnp.mean(f, axis=-1, keepdims=True)
    var = jnp.mean(cen * cen, axis=-1, keepdims=True)
    nrm[...] = (cen * lax.rsqrt(var + 1e-05) * mg_ref[...]).astype(BF)
    routes = routes_ref[...]
    r0, r1 = routes[:, 0:1], routes[:, 1:2]
    lane = lax.broadcasted_iota(jnp.int32, (TOK, 128), 1)
    oh0 = jnp.where(lane == r0, 1.0, 0.0).astype(F32)
    oh1 = jnp.where(lane == r1, 1.0, 0.0).astype(F32)
    before = lax.broadcasted_iota(jnp.int32, (TOK, TOK), 0) > lax.broadcasted_iota(jnp.int32, (TOK, TOK), 1)
    prior = dot(jnp.where(before, 1.0, 0.0).astype(BF), (oh0 + oh1).astype(BF))

    def slot_of(r, oh):
        rank = jnp.sum(prior * oh, axis=1, keepdims=True)
        one = (r & 1).astype(F32)
        grp = (r >> 1).astype(F32)
        low = one * 128.0 + grp * 8.0 + rank
        high = 256.0 + grp * 8.0 + one * 2.0 + rank - 8.0
        return jnp.where(rank < 8.0, low, high)

    s0, s1 = slot_of(r0, oh0), slot_of(r1, oh1)
    sid_s[0] = jnp.broadcast_to(s0, (TOK, 128))
    sid_s[1] = jnp.broadcast_to(s1, (TOK, 128))
    slots = lax.broadcasted_iota(jnp.int32, (TOK, 384), 1).astype(F32)
    sel = jnp.where((slots == s0) | (slots == s1), 1.0, 0.0).astype(BF)
    for n in range(4):
        cols = slice(n * 512, n * 512 + 512)
        got = lax.dot_general(sel, nrm[:, cols], (((0,), (0,)), ((), ())), preferred_element_type=F32)
        out[:, :, cols] = got.reshape(48, 8, 512).astype(BF)

    def rms(ref, gain):
        v = ref[...].astype(F32)
        sq = jnp.mean(v * v, axis=-1, keepdims=True)
        return (v * lax.rsqrt(sq + 1e-06) * gain[...]).astype(BF)

    lat[tp, :, 0:QLAT] = rms(ql_ref, qg_ref)
    lat[tp, :, QLAT:QLAT + KVLAT] = rms(kl_ref, kg_ref)
    lat[tp, :, QLAT + KVLAT:LAT] = kr_ref[...]

    pl.semaphore_wait(barrier, 19)

    def m1(k, c):
        dst = (ep + k) % 16
        for e in range(2):
            remote(out.at[e * 16 + dst], xb.at[y, e, ep], m1_s.at[e], m1_r.at[e], at_ep(dst)).start()
        remote(out.at[32 + dst], bb.at[ep], m1_s.at[2], m1_r.at[2], at_ep(dst)).start()
        return c

    lax.fori_loop(1, 16, m1, 0)
    for e in range(2):
        xb[y, e, ep] = out[e * 16 + ep]
    bb[ep] = out[32 + ep]

    a1 = [remote(lat.at[tp], lat.at[tp], a1_s.at[dy - 1], a1_r.at[dy - 1], at_y(dy)) for dy in (1, 2, 3)]
    for c in (a1[0], a1[2], a1[1]):
        c.start()
    d1 = [remote(lat.at[tp], lat.at[tp], d1_s.at[0], d1_r.at[0], mate)]
    d1[0].start()
    ws = [
        remote(gw_hbm, gw.at[1], w_s.at[0], w_r.at[0], mate),
        remote(uw_hbm, uw.at[1], w_s.at[1], w_r.at[1], mate),
        remote(dw_hbm, dw.at[1], w_s.at[2], w_r.at[2], mate),
        remote(ow_hbm, ow.at[1], w_s.at[3], w_r.at[3], mate),
    ]
    for c in ws:
        c.start()
    for dy in (1, 3, 2):
        a1[dy - 1].wait_recv()
        t = wrap(y - dy) * 2 + core
        c = remote(lat.at[t], lat.at[t], d1_s.at[dy], d1_r.at[dy], mate)
        c.start()
        d1.append(c)
    for c in d1:
        c.wait_recv()

    lane128 = lax.broadcasted_iota(jnp.int32, (HALF // 2, 128), 1)
    lane512 = lax.broadcasted_iota(jnp.int32, (HALF, 128), 1)
    for h in range(2):
        part = lat[h * 4:h * 4 + 4]
        qn = part[:, :, 0:QLAT].reshape(HALF, QLAT)
        kvn = part[:, :, QLAT:QLAT + KVLAT].reshape(HALF, KVLAT)
        rows = slice(h * HALF, h * HALF + HALF)
        qf = dot(qn, wq_ref[...])
        tt = dot(qn, wr_ref[...])
        rot = (tt * ct_ref[rows] + pltpu.roll(tt, 64, 1) * st_ref[rows]).astype(BF)
        zero = jnp.zeros_like(rot)
        qa[rows, 0:128] = qf.astype(BF)
        qb[rows, 0:128] = qf.astype(BF)
        qa[rows, 128:256] = jnp.where(lane512 < 64, rot, zero)
        qb[rows, 128:256] = jnp.where(lane512 < 64, zero, rot)
        kv[h, ep, 0:HALF] = dot(kvn, wk_ref[...]).astype(BF)
        kv[h, ep, HALF:2 * HALF] = dot(kvn, wv_ref[...]).astype(BF)
        lo = part[0:2, :, QLAT + KVLAT:LAT].reshape(HALF // 2, 128)
        hi = part[2:4, :, QLAT + KVLAT:LAT].reshape(HALF // 2, 128)
        kv[h, ep, 2 * HALF:KVR] = jnp.where(lane128 < 64, lo, hi)

    def slot(h, du, dv):
        if h == 0:
            return wrap(z + dv) * 4 + wrap(x + du)
        return wrap(z + du) * 4 + wrap(x + dv)

    pieces = (slice(0, KVH), slice(KVH, KVR))
    signs = (1, -1)
    order = (0, -1, 1, 2)
    P1, P1F, P2, P2F = {}, {}, {}, {}
    for h in range(2):
        for d in range(2):
            sg = signs[d]
            own = kv.at[h, slot(h, 0, 0)]
            P1[h, d] = remote(own, own, p1_s.at[h, d], p1_r.at[h, d], at_ep(slot(h, sg, 0)))
            fw = kv.at[h, slot(h, -sg, 0), pieces[d]]
            P1F[h, d] = remote(fw, fw, p1_s.at[h, 2 + d], p1_r.at[h, 2 + d], at_ep(slot(h, sg, 0)))
            for i in range(4):
                own = kv.at[h, slot(h, order[i], 0)]
                P2[h, i, d] = remote(own, own, p2_s.at[h, i, d], p2_r.at[h, i, d], at_ep(slot(h, 0, sg)))
                fw = kv.at[h, slot(h, order[i], -sg), pieces[d]]
                P2F[h, i, d] = remote(fw, fw, p2_s.at[h, i, 2 + d], p2_r.at[h, i, 2 + d], at_ep(slot(h, 0, sg)))

    for h in range(2):
        for d in range(2):
            P1[h, d].start()
        for d in range(2):
            P2[h, 0, d].start()

    for e in range(2):
        rep = xb.at[y, e, pl.ds(0, 15)]
        remote(rep, rep, m1_s.at[e], m1_r.at[e], mate).wait()
    rep = bb.at[pl.ds(0, 15)]
    remote(rep, rep, m1_s.at[2], m1_r.at[2], mate).wait()
    row64 = lax.broadcasted_iota(jnp.int32, (64, 128), 0)
    col128 = lax.broadcasted_iota(jnp.int32, (64, 128), 1)
    want = ((row64 & 31) >> 1) * 8 + (row64 >> 5) * 2 + (row64 & 1)
    squeeze = jnp.where(want == col128, 1.0, 0.0).astype(BF)
    for n in range(4):
        cols = slice(n * 512, n * 512 + 512)
        both = bb[:, :, cols].reshape(128, 512)
        tight = dot(squeeze, both).reshape(8, 8, 512).astype(BF)
        for e in range(2):
            xb[y, e, 16:20, :, cols] = tight[e * 4:e * 4 + 4]
    X1, X2 = [], []
    for d in range(2):
        X1.append(remote(xb.at[y], xb.at[y], x1_s.at[d], x1_r.at[d], at_y(signs[d])))
        fw = xb.at[wrap(y - signs[d]), d]
        X2.append(remote(fw, fw, x2_s.at[d], x2_r.at[d], at_y(signs[d])))
    for c in X1:
        c.start()

    def step(h, src, qi, masked):
        rows = pl.ds(pl.multiple_of(qi * QT, QT), QT)
        keys0 = kv[h, src, 0:256]
        keys1 = kv[h, src, 256:512]
        rots = kv[h, src, 2 * HALF:KVR]
        vals = kv[h, src, HALF:2 * HALF]
        nt = (((1,), (1,)), ((), ()))
        sa = lax.dot_general(qa[rows], jnp.concatenate([keys0, rots], 1), nt, preferred_element_type=F32)
        sb_ = lax.dot_general(qb[rows], jnp.concatenate([keys1, rots], 1), nt, preferred_element_type=F32)
        s = jnp.concatenate([sa, sb_], 1) * SCALE2
        if masked:
            qp = qi * QT + lax.broadcasted_iota(jnp.int32, (QT, HALF), 0)
            kp = h * HALF + lax.broadcasted_iota(jnp.int32, (QT, HALF), 1)
            s = jnp.where(kp <= qp, s, -1e30)
        old = m_s[rows]
        new = jnp.maximum(old, jnp.max(s, axis=1, keepdims=True))
        p = jnp.exp2(s - new[:, 0:1])
        fac = jnp.exp2(old - new)
        m_s[rows] = new
        l_s[rows] = l_s[rows] * fac + ((p[:, 0:128] + p[:, 128:256]) + (p[:, 256:384] + p[:, 384:512]))
        acc[rows] = acc[rows] * fac + dot(p.astype(BF), vals)

    def attend(h, src):
        @pl.when(src < ep)
        def _():
            lax.fori_loop(0, GROUP // QT, lambda qi, c: (step(h, src, qi, False), c)[1], 0)

    m_s[...] = jnp.full((GROUP, 128), -1e30, F32)
    l_s[...] = jnp.zeros((GROUP, 128), F32)
    acc[...] = jnp.zeros((GROUP, 128), F32)
    lax.fori_loop(0, 4, lambda qi, c: (step(0, ep, qi, True), c)[1], 0)
    lax.fori_loop(2, 4, lambda qi, c: (step(1, ep, qi, True), c)[1], 0)

    for h in range(2):
        for d in range(2):
            P1[h, d].wait_recv()
            P1F[h, d].start()
        for i in (1, 2):
            for d in range(2):
                P2[h, i, d].start()

    for c in locals_:
        c.wait()
    for c in ws:
        c.wait_recv()

    def expert(ys):
        n = len(ys)

        def one(e, c):
            rows = jnp.concatenate([xb[b, e].reshape(160, D) for b in ys], 0)
            total = [None] * 4
            hid = []
            for w in range(2):
                g = jnp.minimum(dot(rows, gw[w, e]), 7.0)
                u = jnp.clip(dot(rows, uw[w, e]), -7.0, 7.0)
                hid.append((g * jax.nn.sigmoid(1.702 * g) * (u + 1.0)).astype(BF))
            both = jnp.concatenate(hid, 1)
            for q in range(4):
                cols = slice(q * 512, q * 512 + 512)
                down = jnp.concatenate([dw[0, e, :, cols], dw[1, e, :, cols]], 0)
                total = dot(both, down).astype(BF)
                for k in range(n):
                    pp[ys[k], e, :, cols] = total[k * 160:k * 160 + 160]
            return c

        lax.fori_loop(0, 2, one, 0)

    def ring(part, a_, b_, c_, s_, ssem, rsem):
        C, A, B = [], [], []
        for d in range(2):
            dev = at_y(signs[d])
            near = wrap(y + signs[d])
            far = wrap(y + 2)
            C.append(remote(part.at[near, 1 - d], c_.at[d], ssem.at[d], rsem.at[d], dev))
            A.append(remote(part.at[far, d], a_.at[d], ssem.at[2 + d], rsem.at[2 + d], dev))
            B.append(remote(s_.at[d], b_.at[d], ssem.at[4 + d], rsem.at[4 + d], dev))
        return C, A, B

    def relay(part, a_, s_, A, B):
        for d in range(2):
            A[d].wait_recv()
            s_[d] = (part[wrap(y + signs[d]), d].astype(F32) + a_[d].astype(F32)).astype(BF)
            B[d].start()

    RC, RA, RB = ring(pp, ra, rb, rc, sb, r_s, r_r)
    TC, TA, TB = ring(pm, ma, mb, mc, ms, t_s, t_r)

    expert([y])

    for h in range(2):
        for d in range(2):
            P1F[h, d].wait_recv()
        for d in range(2):
            P2[h, 3, d].start()
    for h in range(2):
        for du in (-1, 1):
            attend(h, slot(h, du, 0))
    for d in range(2):
        X1[d].wait_recv()
        X2[d].start()
    for h in range(2):
        for d in range(2):
            P2[h, 0, d].wait_recv()
            P2F[h, 0, d].start()
    expert([wrap(y + 1), wrap(y - 1)])
    for c in RC:
        c.start()
    for i in (1, 2):
        for h in range(2):
            for d in range(2):
                P2[h, i, d].wait_recv()
                P2F[h, i, d].start()
    for h in range(2):
        attend(h, slot(h, 2, 0))
        for dv in (-1, 1):
            attend(h, slot(h, 0, dv))
    for c in X2:
        c.wait_recv()
    expert([wrap(y + 2)])
    for c in RA:
        c.start()
    for h in range(2):
        for d in range(2):
            P2[h, 3, d].wait_recv()
            P2F[h, 3, d].start()
    for h in range(2):
        for i in (1, 2):
            for dv in (-1, 1):
                attend(h, slot(h, order[i], dv))
    relay(pp, ra, sb, RA, RB)
    for h in range(2):
        for dv in (-1, 1):
            attend(h, slot(h, 2, dv))
    for i in range(4):
        for h in range(2):
            for d in range(2):
                P2F[h, i, d].wait_recv()
            attend(h, slot(h, order[i], 2))

    for b in range(4):
        for side, dst in ((core, att_loc), (1 - core, att_snd)):
            rows = pl.ds(pl.multiple_of((b * 2 + side) * TOK, TOK), TOK)
            total = jnp.sum(l_s[rows], axis=1, keepdims=True)
            dst[b] = (acc[rows] / total).astype(BF)
    AT = remote(att_snd, att_rcv, at_s, at_r, mate)
    AT.start()
    AT.wait_recv()
    heads = jnp.concatenate([att_loc[...].reshape(HALF, VDIM), att_rcv[...].reshape(HALF, VDIM)], 1)
    for q in range(4):
        cols = slice(q * 512, q * 512 + 512)
        w2 = jnp.concatenate([ow[0, :, cols], ow[1, :, cols]], 0)
        pm[:, :, :, cols] = dot(heads, w2).astype(BF).reshape(4, 2, 64, 512)
    for c in TC + TA:
        c.start()

    final = []
    for e in range(2):
        RC[1 - e].wait_recv()
        RB[e].wait_recv()
        whole = pp[y, e].astype(F32) + rb[e].astype(F32) + rc[1 - e].astype(F32)
        tight = whole.astype(BF)
        final.append(tight[128:160])
        out[e * 16:e * 16 + 16] = tight[0:128].reshape(16, 8, D)
    compact = jnp.concatenate(final, 0)
    for n in range(4):
        cols = slice(n * 512, n * 512 + 512)
        wide = lax.dot_general(
            squeeze, compact[:, cols], (((0,), (0,)), ((), ())), preferred_element_type=F32
        )
        out[32:48, :, cols] = wide.reshape(16, 8, 512).astype(BF)

    def m5(k, c):
        dst = (ep + k) % 16
        for g in range(3):
            remote(out.at[g * 16 + dst], back.at[g * 16 + ep], m5_s.at[g], m5_r.at[g], at_ep(dst)).start()
        return c

    lax.fori_loop(1, 16, m5, 0)
    for g in range(3):
        back[g * 16 + ep] = out[g * 16 + ep]

    relay(pm, ma, ms, TA, TB)

    for g in range(3):
        rep = back.at[pl.ds(g * 16, 15)]
        remote(rep, rep, m5_s.at[g], m5_r.at[g], mate).wait()
    rw = rw_ref[...]
    tot = jnp.sum(rw, axis=1, keepdims=True)
    w0, w1 = rw[:, 0:1] / tot, rw[:, 1:2] / tot
    pick0 = jnp.where(slots == sid_s[0][:, 0:1], 1.0, 0.0).astype(BF)
    pick1 = jnp.where(slots == sid_s[1][:, 0:1], 1.0, 0.0).astype(BF)
    for n in range(4):
        cols = slice(n * 512, n * 512 + 512)
        rows = back[:, :, cols].reshape(384, 512)
        oexp_ref[:, cols] = (w0 * dot(pick0, rows) + w1 * dot(pick1, rows)).astype(BF)

    for e in range(2):
        TC[1 - e].wait_recv()
        TB[e].wait_recv()
        whole = pm[y, e].astype(F32) + mb[e].astype(F32) + mc[1 - e].astype(F32)
        omix_ref[e * 64:e * 64 + 64] = whole.astype(BF)

    for c in a1 + d1 + ws + X1 + X2 + RC + RA + RB + TC + TA + TB + [AT]:
        c.wait_send()
    for group in (P1, P1F, P2, P2F):
        for c in group.values():
            c.wait_send()


def tables(ep):
    half = ROPE // 2
    freq = 1.0 / THETA ** (jnp.arange(half, dtype=F32) * 2.0 / ROPE)
    positions = ep * GROUP + jnp.arange(GROUP, dtype=jnp.int32)
    angle = positions.astype(F32)[:, None] * freq[None, :]
    return jnp.cos(angle), jnp.sin(angle)


def per_device(
    query_latent, kv_latent, rope_key, query_gain, kv_gain, query_nope_w, query_rope_w,
    key_up_w, value_up_w, output_w, expert_in, moe_gain, routes, route_weight, gate_w, up_w, down_w,
):
    ep = lax.axis_index("ep")
    tp = lax.axis_index("tp")
    cosine, sine = tables(ep)
    cc = jnp.concatenate([cosine, cosine, sine, sine], 1)
    ss = jnp.concatenate([sine, sine, cosine, cosine], 1)
    mine = lax.dynamic_slice_in_dim(cc, tp * TOK, TOK, 0)
    cm, sm = mine[:, 0:64], mine[:, 64:128]
    rk = rope_key.astype(F32)
    turned = jnp.concatenate([-rk[:, 32:], rk[:, :32]], 1)
    kr = (rk * cm + turned * sm).astype(BF)
    kr = jnp.concatenate([kr, kr], 1)
    wr = jnp.concatenate([query_rope_w, -query_rope_w[:, 32:], query_rope_w[:, :32]], 1)
    dma = pltpu.SemaphoreType.DMA
    vm = pl.BlockSpec(memory_space=VM)
    hbm = pl.BlockSpec(memory_space=pl.ANY)
    return pl.pallas_call(
        kernel,
        out_shape=(jax.ShapeDtypeStruct((TOK, D), BF), jax.ShapeDtypeStruct((TOK, D), BF)),
        in_specs=[vm] * 15 + [hbm] * 4,
        out_specs=(vm, vm),
        scratch_shapes=[
            VM((8, TOK, LAT), BF), VM((2, 16, KVR, 128), BF), VM((GROUP, 256), BF), VM((GROUP, 256), BF),
            VM((GROUP, 128), F32), VM((GROUP, 128), F32), VM((GROUP, 128), F32),
            VM((4, TOK, 128), BF), VM((4, TOK, 128), BF), VM((4, TOK, 128), BF),
            VM((2, 128, D), BF), VM((2, 2, D, HID), BF), VM((2, 2, D, HID), BF), VM((2, 2, HID, D), BF),
            VM((48, 8, D), BF), VM((4, 2, 20, 8, D), BF), VM((16, 8, D), BF), VM((48, 8, D), BF),
            VM((4, 2, 160, D), BF), VM((2, 160, D), BF), VM((2, 160, D), BF), VM((2, 160, D), BF), VM((2, 160, D), BF),
            VM((4, 2, 64, D), BF), VM((2, 64, D), BF), VM((2, 64, D), BF), VM((2, 64, D), BF), VM((2, 64, D), BF),
            VM((2, TOK, 128), F32), VM((TOK, D), BF),
            dma((4,)), dma((3,)), dma((3,)), dma((4,)), dma((4,)), dma((3,)), dma((3,)), dma((4,)), dma((4,)),
            dma((2, 4)), dma((2, 4)), dma((2, 4, 4)), dma((2, 4, 4)), dma((2,)), dma((2,)), dma((2,)), dma((2,)),
            dma((6,)), dma((6,)), dma((6,)), dma((6,)), dma, dma, dma((3,)), dma((3,)),
        ],
        compiler_params=pltpu.CompilerParams(
            collective_id=0, has_side_effects=True, vmem_limit_bytes=66_000_000
        ),
    )(
        query_latent, kv_latent, kr, query_gain.reshape(1, -1), kv_gain.reshape(1, -1), cc, ss,
        query_nope_w, wr, key_up_w, value_up_w, expert_in, moe_gain.reshape(1, -1), routes, route_weight,
        output_w, gate_w, up_w, down_w,
    )


def solution(mesh):
    rows = P(("ep", "tp"), None)
    placed = (
        rows, rows, rows, P(), P(), P(None, "tp"), P(None, "tp"), P(None, "tp"), P(None, "tp"), P("tp", None),
        rows, P(), rows, rows, P("ep", None, "tp"), P("ep", None, "tp"), P("ep", "tp", None),
    )
    return jax.shard_map(per_device, mesh=mesh, in_specs=placed, out_specs=(rows, rows), check_vma=False)
```

profile of v0, /device:TPU:101, one launch (start us, length us, event | category | flops | bytes accessed | tf_op | source)
XLA Modules:
  0.0 188.7 jit_solution(84320703080136922)
XLA Ops:
  0.6 0.0 copy-start.2
  0.6 0.0 copy-start.1
  0.7 1.9 multiply_cosine_fusion
  2.6 0.0 copy-start.4
  2.6 0.0 copy-start.5
  2.6 0.0 copy-start.3
  2.6 1.7 pad_maximum_fusion.1
  4.3 0.0 copy-start
  4.3 0.0 copy-done.2
  4.3 0.1 copy.19
  4.4 0.1 slice_negate_fusion.1
  4.5 0.1 fusion.1
  4.6 0.7 pad_maximum_fusion.3.kr_ref
  5.3 0.0 copy-done.1
  5.3 0.2 copy.22
  5.5 0.1 slice_negate_fusion
  5.6 0.9 pad_maximum_fusion.2.wr_ref
  6.5 0.0 copy-done.4
  6.5 0.7 copy.23.routes_ref
  7.2 0.0 copy-done.5
  7.2 0.7 copy.24.rw_ref
  8.0 0.0 copy-done.3
  8.0 0.6 reshape.24.qg_ref
  8.5 0.0 copy-done
  8.5 176.4 %shard_map.176 = (bf16[128,2048]{1,0:T(8,128)(2,1)}, bf16[128,2048]{1,0:T(8,128)(2,1)}) custom-call(bf16[128,768]{1,0:T(8,128)(2,1)} %ql_ref.1, bf16[128,512]{1,0:T(8,128)(2,1)} %kl_ref.1, bf16[128,128]{1,0:T(8,128)(2,1)} %pad_maximum_fusion.3.kr_ref, f32[1,768]{1,0:T(1,128)} %reshape.24.qg_ref, f32[1,512]{1,0:T(1,128)} %bitcast.3, f32[1024,128]{1,0:T(8,128)} %copy-done, ...), custom_call_target="tpu_custom_call" | custom-call | tf_op jit(solution)/shard_map/pallas_call | solution.py:469
  185.0 1.9 copy.27
  186.9 1.9 copy.28
  (4 shorter events, 0.0 us)
Async XLA Ops:
  0.6 3.7 %copy-start.2 = (bf16[128,64]{0,1:T(8,128)(2,1)S(1)}, bf16[128,64]{0,1:T(8,128)(2,1)}, u32[]{:S(2)}) copy-start(bf16[128,64]{0,1:T(8,128)(2,1)} %param.19) | copy-start | bytes 49156
  0.6 4.7 %copy-start.1 = (bf16[768,64]{0,1:T(8,128)(2,1)S(1)}, bf16[768,64]{0,1:T(8,128)(2,1)}, u32[]{:S(2)}) copy-start(bf16[768,64]{0,1:T(8,128)(2,1)} %param.23) | copy-start | bytes 294916
  2.6 3.9 %copy-start.4 = (s32[128,2]{0,1:T(2,128)S(1)}, s32[128,2]{0,1:T(2,128)}, u32[]{:S(2)}) copy-start(s32[128,2]{0,1:T(2,128)} %param.29) | copy-start | bytes 3076
  2.6 4.6 %copy-start.5 = (f32[128,2]{0,1:T(2,128)S(1)}, f32[128,2]{0,1:T(2,128)}, u32[]{:S(2)}) copy-start(f32[128,2]{0,1:T(2,128)} %param.30) | copy-start | bytes 3076
  2.6 5.4 %copy-start.3 = (f32[768]{0:T(1024)S(1)}, f32[768]{0:T(1024)}, u32[]{:S(2)}) copy-start(f32[768]{0:T(1024)} %param.20) | copy-start | bytes 9220
  4.3 4.3 %copy-start = (f32[1024,128]{1,0:T(8,128)}, f32[1024,128]{1,0:T(8,128)S(1)}, u32[]{:S(2)}) copy-start(f32[1024,128]{1,0:T(8,128)S(1)} %get-tuple-element.3.ct_ref) | copy-start | bytes 1572868
where the time goes:
time: 189 us
  Pallas kernels  176 us (93%)
  local copies, waits for them, and re-layouts  6.11 us (3%)
  other arithmetic  5.46 us (3%)
    pallas_call x1, Pallas kernels, per_device(): pl.pallas_call(kernel, out_shape=(jax.ShapeDtypeStruct((TOK, D), BF), jax...  176 us
    unnamed x18, local copies, waits for them, and re-layouts  5.53 us

commit v1 on v0

--- a/solution.py
+++ b/solution.py
@@ -3,6 +3,7 @@
 
 import jax
 import jax.numpy as jnp
+import numpy as np
 from jax import lax
 from jax.experimental import pallas as pl
 from jax.experimental.pallas import tpu as pltpu
@@ -31,12 +32,12 @@
 
 
 def kernel(
-    ql_ref, kl_ref, kr_ref, qg_ref, kg_ref, ct_ref, st_ref, wq_ref, wr_ref, wk_ref, wv_ref,
+    ql_ref, kl_ref, rk_ref, qg_ref, kg_ref, tab_ref, wq_ref, wp_ref, wk_ref, wv_ref,
     xin_ref, mg_ref, routes_ref, rw_ref, ow_hbm, gw_hbm, uw_hbm, dw_hbm,
     omix_ref, oexp_ref,
     lat, kv, qa, qb, m_s, l_s, acc, att_loc, att_snd, att_rcv,
     ow, gw, uw, dw,
-    out, xb, bb, back, pp, ra, rb, rc, sb,
+    out, outb, xb, bb, back, backb, pp, ra, rb, rc, sb,
     pm, ma, mb, mc, ms, sid_s, nrm,
     loc_sem, m1_s, m1_r, w_s, w_r, a1_s, a1_r, d1_s, d1_r,
     p1_s, p1_r, p2_s, p2_r, x1_s, x1_r, x2_s, x2_r,
@@ -86,40 +87,66 @@
     cen = f - jnp.mean(f, axis=-1, keepdims=True)
     var = jnp.mean(cen * cen, axis=-1, keepdims=True)
     nrm[...] = (cen * lax.rsqrt(var + 1e-05) * mg_ref[...]).astype(BF)
-    routes = routes_ref[...]
-    r0, r1 = routes[:, 0:1], routes[:, 1:2]
+    rowi = lax.broadcasted_iota(jnp.int32, (TOK, TOK), 0)
+    coli = lax.broadcasted_iota(jnp.int32, (TOK, TOK), 1)
+
+    def column(row):
+        return jnp.sum(jnp.where(rowi == coli, jnp.broadcast_to(row, (TOK, TOK)), 0.0), axis=1, keepdims=True)
+
+    routes = routes_ref[...].astype(F32)
+    r0, r1 = (column(routes[k:k + 1]).astype(jnp.int32) for k in range(2))
     lane = lax.broadcasted_iota(jnp.int32, (TOK, 128), 1)
     oh0 = jnp.where(lane == r0, 1.0, 0.0).astype(F32)
     oh1 = jnp.where(lane == r1, 1.0, 0.0).astype(F32)
-    before = lax.broadcasted_iota(jnp.int32, (TOK, TOK), 0) > lax.broadcasted_iota(jnp.int32, (TOK, TOK), 1)
-    prior = dot(jnp.where(before, 1.0, 0.0).astype(BF), (oh0 + oh1).astype(BF))
+    prior = dot(jnp.where(rowi > coli, 1.0, 0.0).astype(BF), (oh0 + oh1).astype(BF))
 
     def slot_of(r, oh):
         rank = jnp.sum(prior * oh, axis=1, keepdims=True)
         one = (r & 1).astype(F32)
         grp = (r >> 1).astype(F32)
         low = one * 128.0 + grp * 8.0 + rank
-        high = 256.0 + grp * 8.0 + one * 2.0 + rank - 8.0
+        high = 256.0 + grp * 4.0 + one * 2.0 + rank - 8.0
         return jnp.where(rank < 8.0, low, high)
 
     s0, s1 = slot_of(r0, oh0), slot_of(r1, oh1)
     sid_s[0] = jnp.broadcast_to(s0, (TOK, 128))
     sid_s[1] = jnp.broadcast_to(s1, (TOK, 128))
-    slots = lax.broadcasted_iota(jnp.int32, (TOK, 384), 1).astype(F32)
+    slots = lax.broadcasted_iota(jnp.int32, (TOK, 256), 1).astype(F32)
+    slotb = lax.broadcasted_iota(jnp.int32, (TOK, 64), 1).astype(F32) + 256.0
     sel = jnp.where((slots == s0) | (slots == s1), 1.0, 0.0).astype(BF)
+    selb = jnp.where((slotb == s0) | (slotb == s1), 1.0, 0.0).astype(BF)
+    tn = (((0,), (0,)), ((), ()))
     for n in range(4):
         cols = slice(n * 512, n * 512 + 512)
-        got = lax.dot_general(sel, nrm[:, cols], (((0,), (0,)), ((), ())), preferred_element_type=F32)
-        out[:, :, cols] = got.reshape(48, 8, 512).astype(BF)
+        got = lax.dot_general(sel, nrm[:, cols], tn, preferred_element_type=F32)
+        out[:, :, cols] = got.reshape(32, 8, 512).astype(BF)
+        got = lax.dot_general(selb, nrm[:, cols], tn, preferred_element_type=F32)
+        outb[:, :, cols] = got.reshape(16, 4, 512).astype(BF)
 
     def rms(ref, gain):
         v = ref[...].astype(F32)
         sq = jnp.mean(v * v, axis=-1, keepdims=True)
-        return (v * lax.rsqrt(sq + 1e-06) * gain[...]).astype(BF)
-
-    lat[tp, :, 0:QLAT] = rms(ql_ref, qg_ref)
-    lat[tp, :, QLAT:QLAT + KVLAT] = rms(kl_ref, kg_ref)
-    lat[tp, :, QLAT + KVLAT:LAT] = kr_ref[...]
+        return (v * lax.rsqrt(sq + 1e-06) * gain).astype(BF)
+
+    lat[tp, :, 0:QLAT] = rms(ql_ref, qg_ref[...].reshape(1, QLAT))
+    lat[tp, :, QLAT:QLAT + KVLAT] = rms(kl_ref, kg_ref[...])
+    i64 = lax.broadcasted_iota(jnp.int32, (ROPE, 128), 0)
+    j64 = lax.broadcasted_iota(jnp.int32, (ROPE, 128), 1)
+    plain = jnp.where(i64 == j64, 1.0, 0.0) + jnp.where(i64 + 96 == j64, 1.0, 0.0)
+    turn = (plain - jnp.where(i64 + 32 == j64, jnp.where(j64 >= 64, 1.0, 0.0), 0.0)).astype(BF)
+
+    def angles(block):
+        cb, sb0 = tab_ref[0], tab_ref[1]
+        k = [tab_ref[2 + n, pl.ds(block, 1), :] for n in range(4)]
+        return cb * k[0] + sb0 * k[1], cb * k[2] + sb0 * k[3]
+
+    def rotated(both, ct, st):
+        return (both * ct + pltpu.roll(both, 64, 1) * st).astype(BF)
+
+    lat[tp, :, QLAT + KVLAT:LAT] = rotated(
+        lax.dot_general(rk_ref[...], turn, tn, preferred_element_type=F32), *angles(ep * 8 + tp)
+    )
+    wr = lax.dot_general(wp_ref[...], turn, tn, preferred_element_type=F32).astype(BF)
 
     pl.semaphore_wait(barrier, 19)
 
@@ -127,13 +154,13 @@
         dst = (ep + k) % 16
         for e in range(2):
             remote(out.at[e * 16 + dst], xb.at[y, e, ep], m1_s.at[e], m1_r.at[e], at_ep(dst)).start()
-        remote(out.at[32 + dst], bb.at[ep], m1_s.at[2], m1_r.at[2], at_ep(dst)).start()
+        remote(outb.at[dst], bb.at[ep], m1_s.at[2], m1_r.at[2], at_ep(dst)).start()
         return c
 
     lax.fori_loop(1, 16, m1, 0)
     for e in range(2):
         xb[y, e, ep] = out[e * 16 + ep]
-    bb[ep] = out[32 + ep]
+    bb[ep] = outb[ep]
 
     a1 = [remote(lat.at[tp], lat.at[tp], a1_s.at[dy - 1], a1_r.at[dy - 1], at_y(dy)) for dy in (1, 2, 3)]
     for c in (a1[0], a1[2], a1[1]):
@@ -165,8 +192,10 @@
         kvn = part[:, :, QLAT:QLAT + KVLAT].reshape(HALF, KVLAT)
         rows = slice(h * HALF, h * HALF + HALF)
         qf = dot(qn, wq_ref[...])
-        tt = dot(qn, wr_ref[...])
-        rot = (tt * ct_ref[rows] + pltpu.roll(tt, 64, 1) * st_ref[rows]).astype(BF)
+        tabs = [angles(ep * 8 + h * 4 + t) for t in range(4)]
+        rot = rotated(
+            dot(qn, wr), jnp.concatenate([t[0] for t in tabs], 0), jnp.concatenate([t[1] for t in tabs], 0)
+        )
         zero = jnp.zeros_like(rot)
         qa[rows, 0:128] = qf.astype(BF)
         qb[rows, 0:128] = qf.astype(BF)
@@ -211,19 +240,21 @@
         remote(rep, rep, m1_s.at[e], m1_r.at[e], mate).wait()
     rep = bb.at[pl.ds(0, 15)]
     remote(rep, rep, m1_s.at[2], m1_r.at[2], mate).wait()
-    row64 = lax.broadcasted_iota(jnp.int32, (64, 128), 0)
-    col128 = lax.broadcasted_iota(jnp.int32, (64, 128), 1)
-    want = ((row64 & 31) >> 1) * 8 + (row64 >> 5) * 2 + (row64 & 1)
-    squeeze = jnp.where(want == col128, 1.0, 0.0).astype(BF)
+    row64 = lax.broadcasted_iota(jnp.int32, (64, 64), 0)
+    col64 = lax.broadcasted_iota(jnp.int32, (64, 64), 1)
+    want = ((row64 & 31) >> 1) * 4 + (row64 >> 5) * 2 + (row64 & 1)
+    squeeze = jnp.where(want == col64, 1.0, 0.0).astype(BF)
     for n in range(4):
         cols = slice(n * 512, n * 512 + 512)
-        both = bb[:, :, cols].reshape(128, 512)
+        both = bb[:, :, cols].reshape(64, 512)
         tight = dot(squeeze, both).reshape(8, 8, 512).astype(BF)
         for e in range(2):
             xb[y, e, 16:20, :, cols] = tight[e * 4:e * 4 + 4]
-    X1, X2 = [], []
+    X1, XL, X2 = [], [], []
     for d in range(2):
-        X1.append(remote(xb.at[y], xb.at[y], x1_s.at[d], x1_r.at[d], at_y(signs[d])))
+        first, last = xb.at[y, d], xb.at[y, 1 - d]
+        X1.append(remote(first, first, x1_s.at[d], x1_r.at[d], at_y(signs[d])))
+        XL.append(remote(last, last, x1_s.at[2 + d], x1_r.at[2 + d], at_y(signs[d])))
         fw = xb.at[wrap(y - signs[d]), d]
         X2.append(remote(fw, fw, x2_s.at[d], x2_r.at[d], at_y(signs[d])))
     for c in X1:
@@ -262,18 +293,8 @@
     lax.fori_loop(0, 4, lambda qi, c: (step(0, ep, qi, True), c)[1], 0)
     lax.fori_loop(2, 4, lambda qi, c: (step(1, ep, qi, True), c)[1], 0)
 
-    for h in range(2):
-        for d in range(2):
-            P1[h, d].wait_recv()
-            P1F[h, d].start()
-        for i in (1, 2):
-            for d in range(2):
-                P2[h, i, d].start()
-
-    for c in locals_:
-        c.wait()
-    for c in ws:
-        c.wait_recv()
+    for c in XL:
+        c.start()
 
     def expert(ys):
         n = len(ys)
@@ -298,76 +319,107 @@
         lax.fori_loop(0, 2, one, 0)
 
     def ring(part, a_, b_, c_, s_, ssem, rsem):
+        n = part.shape[2] // 2
         C, A, B = [], [], []
         for d in range(2):
             dev = at_y(signs[d])
             near = wrap(y + signs[d])
             far = wrap(y + 2)
             C.append(remote(part.at[near, 1 - d], c_.at[d], ssem.at[d], rsem.at[d], dev))
-            A.append(remote(part.at[far, d], a_.at[d], ssem.at[2 + d], rsem.at[2 + d], dev))
-            B.append(remote(s_.at[d], b_.at[d], ssem.at[4 + d], rsem.at[4 + d], dev))
+            for k in range(2):
+                q = pl.ds(k * n, n)
+                m = 2 + d * 2 + k
+                A.append(remote(part.at[far, d, q], a_.at[d, q], ssem.at[m], rsem.at[m], dev))
+                m = 6 + d * 2 + k
+                B.append(remote(s_.at[d, q], b_.at[d, q], ssem.at[m], rsem.at[m], dev))
         return C, A, B
 
-    def relay(part, a_, s_, A, B):
+    def relay(part, a_, s_, A, B, k):
+        n = part.shape[2] // 2
+        q = slice(k * n, k * n + n)
         for d in range(2):
-            A[d].wait_recv()
-            s_[d] = (part[wrap(y + signs[d]), d].astype(F32) + a_[d].astype(F32)).astype(BF)
-            B[d].start()
+            A[d * 2 + k].wait_recv()
+            s_[d, q] = (part[wrap(y + signs[d]), d, q].astype(F32) + a_[d, q].astype(F32)).astype(BF)
+            B[d * 2 + k].start()
 
     RC, RA, RB = ring(pp, ra, rb, rc, sb, r_s, r_r)
     TC, TA, TB = ring(pm, ma, mb, mc, ms, t_s, t_r)
 
+    def p1_on():
+        for h in range(2):
+            for d in range(2):
+                P1[h, d].wait_recv()
+                P1F[h, d].start()
+        for h in range(2):
+            for i in (1, 2):
+                for d in range(2):
+                    P2[h, i, d].start()
+
+    def p2_on(i):
+        for h in range(2):
+            for d in range(2):
+                P2[h, i, d].wait_recv()
+                P2F[h, i, d].start()
+
+    def p1f_on():
+        for h in range(2):
+            for d in range(2):
+                P1F[h, d].wait_recv()
+        for h in range(2):
+            for d in range(2):
+                P2[h, 3, d].start()
+
+    def near(i):
+        for h in range(2):
+            for dv in (-1, 1):
+                attend(h, slot(h, order[i], dv))
+
+    def far(i):
+        for h in range(2):
+            for d in range(2):
+                P2F[h, i, d].wait_recv()
+            attend(h, slot(h, order[i], 2))
+
+    for c in locals_:
+        c.wait()
+    for c in ws:
+        c.wait_recv()
     expert([y])
-
-    for h in range(2):
-        for d in range(2):
-            P1F[h, d].wait_recv()
-        for d in range(2):
-            P2[h, 3, d].start()
+    p1_on()
+    p2_on(0)
+    for c in X1:
+        c.wait_recv()
+    for c in X2:
+        c.start()
     for h in range(2):
         for du in (-1, 1):
             attend(h, slot(h, du, 0))
-    for d in range(2):
-        X1[d].wait_recv()
-        X2[d].start()
-    for h in range(2):
-        for d in range(2):
-            P2[h, 0, d].wait_recv()
-            P2F[h, 0, d].start()
+    near(0)
+    for c in XL:
+        c.wait_recv()
     expert([wrap(y + 1), wrap(y - 1)])
     for c in RC:
         c.start()
-    for i in (1, 2):
-        for h in range(2):
-            for d in range(2):
-                P2[h, i, d].wait_recv()
-                P2F[h, i, d].start()
+    p1f_on()
+    p2_on(1)
+    p2_on(2)
     for h in range(2):
         attend(h, slot(h, 2, 0))
-        for dv in (-1, 1):
-            attend(h, slot(h, 0, dv))
+    near(1)
     for c in X2:
         c.wait_recv()
     expert([wrap(y + 2)])
-    for c in RA:
-        c.start()
-    for h in range(2):
-        for d in range(2):
-            P2[h, 3, d].wait_recv()
-            P2F[h, 3, d].start()
-    for h in range(2):
-        for i in (1, 2):
-            for dv in (-1, 1):
-                attend(h, slot(h, order[i], dv))
-    relay(pp, ra, sb, RA, RB)
-    for h in range(2):
-        for dv in (-1, 1):
-            attend(h, slot(h, 2, dv))
-    for i in range(4):
-        for h in range(2):
-            for d in range(2):
-                P2F[h, i, d].wait_recv()
-            attend(h, slot(h, order[i], 2))
+    for k in (0, 2, 1, 3):
+        RA[k].start()
+    near(2)
+    p2_on(3)
+    near(3)
+    far(0)
+    relay(pp, ra, sb, RA, RB, 0)
+    far(1)
+    relay(pp, ra, sb, RA, RB, 1)
+    far(2)
+    far(3)
 
     for b in range(4):
         for side, dst in ((core, att_loc), (1 - core, att_snd)):
@@ -382,13 +434,16 @@
         cols = slice(q * 512, q * 512 + 512)
         w2 = jnp.concatenate([ow[0, :, cols], ow[1, :, cols]], 0)
         pm[:, :, :, cols] = dot(heads, w2).astype(BF).reshape(4, 2, 64, 512)
-    for c in TC + TA:
-        c.start()
+    for c in TC:
+        c.start()
+    for k in (0, 2, 1, 3):
+        TA[k].start()
 
     final = []
     for e in range(2):
         RC[1 - e].wait_recv()
-        RB[e].wait_recv()
+        RB[e * 2].wait_recv()
+        RB[e * 2 + 1].wait_recv()
         whole = pp[y, e].astype(F32) + rb[e].astype(F32) + rc[1 - e].astype(F32)
         tight = whole.astype(BF)
         final.append(tight[128:160])
@@ -396,100 +451,99 @@
     compact = jnp.concatenate(final, 0)
     for n in range(4):
         cols = slice(n * 512, n * 512 + 512)
-        wide = lax.dot_general(
-            squeeze, compact[:, cols], (((0,), (0,)), ((), ())), preferred_element_type=F32
-        )
-        out[32:48, :, cols] = wide.reshape(16, 8, 512).astype(BF)
+        wide = lax.dot_general(squeeze, compact[:, cols], tn, preferred_element_type=F32)
+        outb[:, :, cols] = wide.reshape(16, 4, 512).astype(BF)
 
     def m5(k, c):
         dst = (ep + k) % 16
-        for g in range(3):
+        for g in range(2):
             remote(out.at[g * 16 + dst], back.at[g * 16 + ep], m5_s.at[g], m5_r.at[g], at_ep(dst)).start()
+        remote(outb.at[dst], backb.at[ep], m5_s.at[2], m5_r.at[2], at_ep(dst)).start()
         return c
 
     lax.fori_loop(1, 16, m5, 0)
-    for g in range(3):
+    for g in range(2):
         back[g * 16 + ep] = out[g * 16 + ep]
-
-    relay(pm, ma, ms, TA, TB)
-
-    for g in range(3):
+    backb[ep] = outb[ep]
+
+    relay(pm, ma, ms, TA, TB, 0)
+    relay(pm, ma, ms, TA, TB, 1)
+
+    for g in range(2):
         rep = back.at[pl.ds(g * 16, 15)]
         remote(rep, rep, m5_s.at[g], m5_r.at[g], mate).wait()
+    rep = backb.at[pl.ds(0, 15)]
+    remote(rep, rep, m5_s.at[2], m5_r.at[2], mate).wait()
     rw = rw_ref[...]
-    tot = jnp.sum(rw, axis=1, keepdims=True)
-    w0, w1 = rw[:, 0:1] / tot, rw[:, 1:2] / tot
-    pick0 = jnp.where(slots == sid_s[0][:, 0:1], 1.0, 0.0).astype(BF)
-    pick1 = jnp.where(slots == sid_s[1][:, 0:1], 1.0, 0.0).astype(BF)
+    share = rw / jnp.sum(rw, axis=0, keepdims=True)
+    w0, w1 = column(share[0:1]), column(share[1:2])
+    picks = [
+        [jnp.where(c == sid_s[k][:, 0:1], 1.0, 0.0).astype(BF) for c in (slots, slotb)] for k in range(2)
+    ]
     for n in range(4):
         cols = slice(n * 512, n * 512 + 512)
-        rows = back[:, :, cols].reshape(384, 512)
-        oexp_ref[:, cols] = (w0 * dot(pick0, rows) + w1 * dot(pick1, rows)).astype(BF)
+        rows = back[:, :, cols].reshape(256, 512)
+        more = backb[:, :, cols].reshape(64, 512)
+        got = [dot(pick[0], rows) + dot(pick[1], more) for pick in picks]
+        oexp_ref[:, cols] = (w0 * got[0] + w1 * got[1]).astype(BF)
 
     for e in range(2):
         TC[1 - e].wait_recv()
-        TB[e].wait_recv()
+        TB[e * 2].wait_recv()
+        TB[e * 2 + 1].wait_recv()
         whole = pm[y, e].astype(F32) + mb[e].astype(F32) + mc[1 - e].astype(F32)
         omix_ref[e * 64:e * 64 + 64] = whole.astype(BF)
 
-    for c in a1 + d1 + ws + X1 + X2 + RC + RA + RB + TC + TA + TB + [AT]:
+    for c in a1 + d1 + ws + X1 + XL + X2 + RC + RA + RB + TC + TA + TB + [AT]:
         c.wait_send()
     for group in (P1, P1F, P2, P2F):
         for c in group.values():
             c.wait_send()
 
 
-def tables(ep):
-    half = ROPE // 2
-    freq = 1.0 / THETA ** (jnp.arange(half, dtype=F32) * 2.0 / ROPE)
-    positions = ep * GROUP + jnp.arange(GROUP, dtype=jnp.int32)
-    angle = positions.astype(F32)[:, None] * freq[None, :]
-    return jnp.cos(angle), jnp.sin(angle)
+def tables():
+    freq = 1.0 / THETA ** (np.arange(ROPE // 2) * 2.0 / ROPE)
+    inner = np.tile(np.arange(TOK)[:, None] * freq, (1, 4))
+    first = np.tile(TOK * np.arange(128)[:, None] * freq, (1, 2))
+    c, s = np.cos(first), np.sin(first)
+    blocks = [[c, s], [-s, c], [s, c], [c, -s]]
+    return np.stack(
+        [np.cos(inner), np.sin(inner)] + [np.concatenate(b, 1) for b in blocks]
+    ).astype(np.float32)
 
 
 def per_device(
     query_latent, kv_latent, rope_key, query_gain, kv_gain, query_nope_w, query_rope_w,
     key_up_w, value_up_w, output_w, expert_in, moe_gain, routes, route_weight, gate_w, up_w, down_w,
 ):
-    ep = lax.axis_index("ep")
-    tp = lax.axis_index("tp")
-    cosine, sine = tables(ep)
-    cc = jnp.concatenate([cosine, cosine, sine, sine], 1)
-    ss = jnp.concatenate([sine, sine, cosine, cosine], 1)
-    mine = lax.dynamic_slice_in_dim(cc, tp * TOK, TOK, 0)
-    cm, sm = mine[:, 0:64], mine[:, 64:128]
-    rk = rope_key.astype(F32)
-    turned = jnp.concatenate([-rk[:, 32:], rk[:, :32]], 1)
-    kr = (rk * cm + turned * sm).astype(BF)
-    kr = jnp.concatenate([kr, kr], 1)
-    wr = jnp.concatenate([query_rope_w, -query_rope_w[:, 32:], query_rope_w[:, :32]], 1)
     dma = pltpu.SemaphoreType.DMA
     vm = pl.BlockSpec(memory_space=VM)
     hbm = pl.BlockSpec(memory_space=pl.ANY)
     return pl.pallas_call(
         kernel,
         out_shape=(jax.ShapeDtypeStruct((TOK, D), BF), jax.ShapeDtypeStruct((TOK, D), BF)),
-        in_specs=[vm] * 15 + [hbm] * 4,
+        in_specs=[vm] * 14 + [hbm] * 4,
         out_specs=(vm, vm),
         scratch_shapes=[
             VM((8, TOK, LAT), BF), VM((2, 16, KVR, 128), BF), VM((GROUP, 256), BF), VM((GROUP, 256), BF),
             VM((GROUP, 128), F32), VM((GROUP, 128), F32), VM((GROUP, 128), F32),
             VM((4, TOK, 128), BF), VM((4, TOK, 128), BF), VM((4, TOK, 128), BF),
             VM((2, 128, D), BF), VM((2, 2, D, HID), BF), VM((2, 2, D, HID), BF), VM((2, 2, HID, D), BF),
-            VM((48, 8, D), BF), VM((4, 2, 20, 8, D), BF), VM((16, 8, D), BF), VM((48, 8, D), BF),
+            VM((32, 8, D), BF), VM((16, 4, D), BF), VM((4, 2, 20, 8, D), BF), VM((16, 4, D), BF), VM((32, 8, D), BF),
+            VM((16, 4, D), BF),
             VM((4, 2, 160, D), BF), VM((2, 160, D), BF), VM((2, 160, D), BF), VM((2, 160, D), BF), VM((2, 160, D), BF),
             VM((4, 2, 64, D), BF), VM((2, 64, D), BF), VM((2, 64, D), BF), VM((2, 64, D), BF), VM((2, 64, D), BF),
             VM((2, TOK, 128), F32), VM((TOK, D), BF),
             dma((4,)), dma((3,)), dma((3,)), dma((4,)), dma((4,)), dma((3,)), dma((3,)), dma((4,)), dma((4,)),
-            dma((2, 4)), dma((2, 4)), dma((2, 4, 4)), dma((2, 4, 4)), dma((2,)), dma((2,)), dma((2,)), dma((2,)),
-            dma((6,)), dma((6,)), dma((6,)), dma((6,)), dma, dma, dma((3,)), dma((3,)),
+            dma((2, 4)), dma((2, 4)), dma((2, 4, 4)), dma((2, 4, 4)), dma((4,)), dma((4,)), dma((2,)), dma((2,)),
+            dma((10,)), dma((10,)), dma((10,)), dma((10,)), dma, dma, dma((3,)), dma((3,)),
         ],
         compiler_params=pltpu.CompilerParams(
             collective_id=0, has_side_effects=True, vmem_limit_bytes=66_000_000
         ),
     )(
-        query_latent, kv_latent, kr, query_gain.reshape(1, -1), kv_gain.reshape(1, -1), cc, ss,
-        query_nope_w, wr, key_up_w, value_up_w, expert_in, moe_gain.reshape(1, -1), routes, route_weight,
+        query_latent, kv_latent, rope_key.T, query_gain, kv_gain.reshape(1, -1), jnp.asarray(tables()),
+        query_nope_w, query_rope_w.T, key_up_w, value_up_w, expert_in, moe_gain.reshape(1, -1), routes.T, route_weight.T,
         output_w, gate_w, up_w, down_w,
     )
 

time: 189 us -> 154 us (0.81)
  the two profiles are of different devices: /device:TPU:101 before, /device:TPU:102 now
where the time goes in v1:
time: 154 us
  Pallas kernels  150 us (97%)
  local copies, waits for them, and re-layouts  3.76 us (2%)
    pallas_call x1, Pallas kernels, per_device(): pl.pallas_call(kernel, out_shape=(jax.ShapeDtypeStruct((TOK, D), BF), jax...  150 us
    unnamed x2, local copies, waits for them, and re-layouts  3.76 us

profile of v1, /device:TPU:102, one launch (start us, length us, event | category | flops | bytes accessed | tf_op | source)
XLA Modules:
  0.0 154.0 jit_solution(18195359828337057549)
XLA Ops:
  0.6 149.6 %shard_map.185 = (bf16[128,2048]{1,0:T(8,128)(2,1)}, bf16[128,2048]{1,0:T(8,128)(2,1)}) custom-call(bf16[128,768]{1,0:T(8,128)(2,1)} %ql_ref.1, bf16[128,512]{1,0:T(8,128)(2,1)} %kl_ref.1, bf16[64,128]{1,0:T(8,128)(2,1)} %bitcast.7, f32[768]{0:T(1024)} %qg_ref.1, f32[1,512]{1,0:T(1,128)} %bitcast.9, f32[6,128,128]{2,1,0:T(8,128)} %constant.2.clone.tab_ref, ...), custom_call_target="tpu_custom_call" | custom-call | tf_op jit(solution)/shard_map/pallas_call | solution.py:522
  150.2 1.9 %copy.22 = bf16[128,2048]{1,0:T(8,128)(2,1)} copy(bf16[128,2048]{1,0:T(8,128)(2,1)} %get-tuple-element.4) | data formatting | bytes 1048576
  152.1 1.9 %copy.23 = bf16[128,2048]{1,0:T(8,128)(2,1)} copy(bf16[128,2048]{1,0:T(8,128)(2,1)} %get-tuple-element.5) | data formatting | bytes 1048576

commit v2 on v1

--- a/solution.py
+++ b/solution.py
@@ -181,60 +181,7 @@
         c = remote(lat.at[t], lat.at[t], d1_s.at[dy], d1_r.at[dy], mate)
         c.start()
         d1.append(c)
-    for c in d1:
-        c.wait_recv()
-
-    lane128 = lax.broadcasted_iota(jnp.int32, (HALF // 2, 128), 1)
-    lane512 = lax.broadcasted_iota(jnp.int32, (HALF, 128), 1)
-    for h in range(2):
-        part = lat[h * 4:h * 4 + 4]
-        qn = part[:, :, 0:QLAT].reshape(HALF, QLAT)
-        kvn = part[:, :, QLAT:QLAT + KVLAT].reshape(HALF, KVLAT)
-        rows = slice(h * HALF, h * HALF + HALF)
-        qf = dot(qn, wq_ref[...])
-        tabs = [angles(ep * 8 + h * 4 + t) for t in range(4)]
-        rot = rotated(
-            dot(qn, wr), jnp.concatenate([t[0] for t in tabs], 0), jnp.concatenate([t[1] for t in tabs], 0)
-        )
-        zero = jnp.zeros_like(rot)
-        qa[rows, 0:128] = qf.astype(BF)
-        qb[rows, 0:128] = qf.astype(BF)
-        qa[rows, 128:256] = jnp.where(lane512 < 64, rot, zero)
-        qb[rows, 128:256] = jnp.where(lane512 < 64, zero, rot)
-        kv[h, ep, 0:HALF] = dot(kvn, wk_ref[...]).astype(BF)
-        kv[h, ep, HALF:2 * HALF] = dot(kvn, wv_ref[...]).astype(BF)
-        lo = part[0:2, :, QLAT + KVLAT:LAT].reshape(HALF // 2, 128)
-        hi = part[2:4, :, QLAT + KVLAT:LAT].reshape(HALF // 2, 128)
-        kv[h, ep, 2 * HALF:KVR] = jnp.where(lane128 < 64, lo, hi)
-
-    def slot(h, du, dv):
-        if h == 0:
-            return wrap(z + dv) * 4 + wrap(x + du)
-        return wrap(z + du) * 4 + wrap(x + dv)
-
-    pieces = (slice(0, KVH), slice(KVH, KVR))
     signs = (1, -1)
-    order = (0, -1, 1, 2)
-    P1, P1F, P2, P2F = {}, {}, {}, {}
-    for h in range(2):
-        for d in range(2):
-            sg = signs[d]
-            own = kv.at[h, slot(h, 0, 0)]
-            P1[h, d] = remote(own, own, p1_s.at[h, d], p1_r.at[h, d], at_ep(slot(h, sg, 0)))
-            fw = kv.at[h, slot(h, -sg, 0), pieces[d]]
-            P1F[h, d] = remote(fw, fw, p1_s.at[h, 2 + d], p1_r.at[h, 2 + d], at_ep(slot(h, sg, 0)))
-            for i in range(4):
-                own = kv.at[h, slot(h, order[i], 0)]
-                P2[h, i, d] = remote(own, own, p2_s.at[h, i, d], p2_r.at[h, i, d], at_ep(slot(h, 0, sg)))
-                fw = kv.at[h, slot(h, order[i], -sg), pieces[d]]
-                P2F[h, i, d] = remote(fw, fw, p2_s.at[h, i, 2 + d], p2_r.at[h, i, 2 + d], at_ep(slot(h, 0, sg)))
-
-    for h in range(2):
-        for d in range(2):
-            P1[h, d].start()
-        for d in range(2):
-            P2[h, 0, d].start()
-
     for e in range(2):
         rep = xb.at[y, e, pl.ds(0, 15)]
         remote(rep, rep, m1_s.at[e], m1_r.at[e], mate).wait()
@@ -260,39 +207,125 @@
     for c in X1:
         c.start()
 
-    def step(h, src, qi, masked):
-        rows = pl.ds(pl.multiple_of(qi * QT, QT), QT)
-        keys0 = kv[h, src, 0:256]
-        keys1 = kv[h, src, 256:512]
+    for c in d1:
+        c.wait_recv()
+
+    lane128 = lax.broadcasted_iota(jnp.int32, (HALF // 2, 128), 1)
+    lane512 = lax.broadcasted_iota(jnp.int32, (HALF, 128), 1)
+    for h in range(2):
+        part = lat[h * 4:h * 4 + 4]
+        qn = part[:, :, 0:QLAT].reshape(HALF, QLAT)
+        kvn = part[:, :, QLAT:QLAT + KVLAT].reshape(HALF, KVLAT)
+        rows = slice(h * HALF, h * HALF + HALF)
+        qf = dot(qn, wq_ref[...])
+        tabs = [angles(ep * 8 + h * 4 + t) for t in range(4)]
+        rot = rotated(
+            dot(qn, wr), jnp.concatenate([t[0] for t in tabs], 0), jnp.concatenate([t[1] for t in tabs], 0)
+        )
+        zero = jnp.zeros_like(rot)
+        qa[rows, 0:128] = qf.astype(BF)
+        qb[rows, 0:128] = qf.astype(BF)
+        qa[rows, 128:256] = jnp.where(lane512 < 64, rot, zero)
+        qb[rows, 128:256] = jnp.where(lane512 < 64, zero, rot)
+        kv[h, ep, 0:HALF] = dot(kvn, wk_ref[...]).astype(BF)
+        turned = jnp.transpose(dot(kvn, wv_ref[...])).astype(BF)
+        for t in range(4):
+            kv[h, ep, HALF + t * 128:HALF + t * 128 + 128] = turned[:, t * 128:t * 128 + 128]
+        lo = part[0:2, :, QLAT + KVLAT:LAT].reshape(HALF // 2, 128)
+        hi = part[2:4, :, QLAT + KVLAT:LAT].reshape(HALF // 2, 128)
+        kv[h, ep, 2 * HALF:KVR] = jnp.where(lane128 < 64, lo, hi)
+
+    def slot(h, du, dv):
+        if h == 0:
+            return wrap(z + dv) * 4 + wrap(x + du)
+        return wrap(z + du) * 4 + wrap(x + dv)
+
+    pieces = (slice(0, KVH), slice(KVH, KVR))
+    order = (0, -1, 1, 2)
+    P1, P1F, P2, P2F = {}, {}, {}, {}
+    for h in range(2):
+        for d in range(2):
+            sg = signs[d]
+            own = kv.at[h, slot(h, 0, 0)]
+            P1[h, d] = remote(own, own, p1_s.at[h, d], p1_r.at[h, d], at_ep(slot(h, sg, 0)))
+            fw = kv.at[h, slot(h, -sg, 0), pieces[d]]
+            P1F[h, d] = remote(fw, fw, p1_s.at[h, 2 + d], p1_r.at[h, 2 + d], at_ep(slot(h, sg, 0)))
+            for i in range(4):
+                own = kv.at[h, slot(h, order[i], 0)]
+                P2[h, i, d] = remote(own, own, p2_s.at[h, i, d], p2_r.at[h, i, d], at_ep(slot(h, 0, sg)))
+                fw = kv.at[h, slot(h, order[i], -sg), pieces[d]]
+                P2F[h, i, d] = remote(fw, fw, p2_s.at[h, i, 2 + d], p2_r.at[h, i, 2 + d], at_ep(slot(h, 0, sg)))
+
+    for h in range(2):
+        for d in range(2):
+            P1[h, d].start()
+
+    nt = (((1,), (1,)), ((), ()))
+
+    def tile(qi):
+        return pl.ds(qi * QT, QT)
+
+    def scores(h, src, qi, masked):
         rots = kv[h, src, 2 * HALF:KVR]
-        vals = kv[h, src, HALF:2 * HALF]
-        nt = (((1,), (1,)), ((), ()))
-        sa = lax.dot_general(qa[rows], jnp.concatenate([keys0, rots], 1), nt, preferred_element_type=F32)
-        sb_ = lax.dot_general(qb[rows], jnp.concatenate([keys1, rots], 1), nt, preferred_element_type=F32)
-        s = jnp.concatenate([sa, sb_], 1) * SCALE2
+        low = jnp.concatenate([kv[h, src, 0:256], rots], 1)
+        high = jnp.concatenate([kv[h, src, 256:512], rots], 1)
+        s = jnp.concatenate(
+            [
+                lax.dot_general(low, qa[tile(qi)], nt, preferred_element_type=F32),
+                lax.dot_general(high, qb[tile(qi)], nt, preferred_element_type=F32),
+            ],
+            0,
+        )
         if masked:
-            qp = qi * QT + lax.broadcasted_iota(jnp.int32, (QT, HALF), 0)
-            kp = h * HALF + lax.broadcasted_iota(jnp.int32, (QT, HALF), 1)
+            kp = h * HALF + lax.broadcasted_iota(jnp.int32, (HALF, QT), 0)
+            qp = qi * QT + lax.broadcasted_iota(jnp.int32, (HALF, QT), 1)
             s = jnp.where(kp <= qp, s, -1e30)
-        old = m_s[rows]
-        new = jnp.maximum(old, jnp.max(s, axis=1, keepdims=True))
-        p = jnp.exp2(s - new[:, 0:1])
-        fac = jnp.exp2(old - new)
-        m_s[rows] = new
-        l_s[rows] = l_s[rows] * fac + ((p[:, 0:128] + p[:, 128:256]) + (p[:, 256:384] + p[:, 384:512]))
-        acc[rows] = acc[rows] * fac + dot(p.astype(BF), vals)
-
-    def attend(h, src):
-        @pl.when(src < ep)
-        def _():
-            lax.fori_loop(0, GROUP // QT, lambda qi, c: (step(h, src, qi, False), c)[1], 0)
-
-    m_s[...] = jnp.full((GROUP, 128), -1e30, F32)
-    l_s[...] = jnp.zeros((GROUP, 128), F32)
-    acc[...] = jnp.zeros((GROUP, 128), F32)
-    lax.fori_loop(0, 4, lambda qi, c: (step(0, ep, qi, True), c)[1], 0)
-    lax.fori_loop(2, 4, lambda qi, c: (step(1, ep, qi, True), c)[1], 0)
-
+        return s
+
+    def weigh(s, qi):
+        old = m_s[:, tile(qi)]
+        new = jnp.maximum(old, jnp.max(s, axis=0, keepdims=True))
+        p = jnp.exp2((s - new[0:1]) * SCALE2)
+        fac = jnp.exp2((old - new) * SCALE2)
+        m_s[:, tile(qi)] = new
+        l_s[:, tile(qi)] = l_s[:, tile(qi)] * fac + jnp.sum(p.reshape(HALF // 8, 8, QT), axis=0)
+        return p.astype(BF), fac
+
+    def gather_values(p, fac, h, src, qi):
+        vals = jnp.concatenate([kv[h, src, HALF + t * 128:HALF + t * 128 + 128] for t in range(4)], 1)
+        acc[:, tile(qi)] = acc[:, tile(qi)] * fac[0:1] + dot(vals, p)
+
+    def run(items):
+        s, prev = scores(*items[0]), None
+        for n, (h, src, qi, _) in enumerate(items):
+            later = scores(*items[n + 1]) if n + 1 < len(items) else None
+            weighed = weigh(s, qi)
+            if prev is not None:
+                gather_values(*prev)
+            prev, s = weighed + (h, src, qi), later
+        gather_values(*prev)
+
+    def attend_all(count, place):
+        def one(n, c):
+            h, du, dv = place(n)
+            src = wrap(z + dv + h * (du - dv)) * 4 + wrap(x + du + h * (dv - du))
+
+            @pl.when(src < ep)
+            def _():
+                run([(h, src, qi, False) for qi in range(GROUP // QT)])
+
+            return c
+
+        lax.fori_loop(0, count, one, 0)
+
+    m_s[...] = jnp.full((8, GROUP), -1e30, F32)
+    l_s[...] = jnp.zeros((8, GROUP), F32)
+    acc[...] = jnp.zeros((VDIM, GROUP), F32)
+    run([(0, ep, 0, True), (0, ep, 1, True), (0, ep, 2, False), (0, ep, 3, False), (1, ep, 2, True), (1, ep, 3, True)])
+
+    for h in range(2):
+        for d in range(2):
+            P2[h, 0, d].start()
     for c in XL:
         c.start()
 
@@ -369,16 +402,15 @@
             for d in range(2):
                 P2[h, 3, d].start()
 
-    def near(i):
-        for h in range(2):
-            for dv in (-1, 1):
-                attend(h, slot(h, order[i], dv))
+    def near(i, *halves):
+        first = halves[0] if halves else 0
+        attend_all(2 if halves else 4, lambda n: (first + n // 2, order[i], n % 2 * 2 - 1))
 
     def far(i):
         for h in range(2):
             for d in range(2):
                 P2F[h, i, d].wait_recv()
-            attend(h, slot(h, order[i], 2))
+        attend_all(2, lambda n: (n, order[i], 2))
 
     for c in locals_:
         c.wait()
@@ -391,10 +423,7 @@
         c.wait_recv()
     for c in X2:
         c.start()
-    for h in range(2):
-        for du in (-1, 1):
-            attend(h, slot(h, du, 0))
-    near(0)
+    attend_all(8, lambda n: (n // 4, (1 - n // 2 % 2) * (n % 2 * 2 - 1), n // 2 % 2 * (n % 2 * 2 - 1)))
     for c in XL:
         c.wait_recv()
     expert([wrap(y + 1), wrap(y - 1)])
@@ -403,8 +432,7 @@
     p1f_on()
     p2_on(1)
     p2_on(2)
-    for h in range(2):
-        attend(h, slot(h, 2, 0))
+    attend_all(2, lambda n: (n, 2, 0))
     near(1)
     for c in X2:
         c.wait_recv()
@@ -413,27 +441,53 @@
         RA[k].start()
     near(2)
     p2_on(3)
-    near(3)
+    near(3, 0)
+    relay(pp, ra, sb, RA, RB, 0)
+    near(3, 1)
     far(0)
-    relay(pp, ra, sb, RA, RB, 0)
+    relay(pp, ra, sb, RA, RB, 1)
     far(1)
-    relay(pp, ra, sb, RA, RB, 1)
     far(2)
+
+    def finish(e, k):
+        if k == 0:
+            RC[1 - e].wait_recv()
+        RB[e * 2 + k].wait_recv()
+        q = slice(k * 80, k * 80 + 80)
+        return (pp[y, e, q].astype(F32) + rb[e, q].astype(F32) + rc[1 - e, q].astype(F32)).astype(BF)
+
+    def send_back(first, count):
+        def one(k, c):
+            dst = first + (ep + k) % count
+
+            @pl.when(dst != ep)
+            def _():
+                for g in range(2):
+                    remote(out.at[g * 16 + dst], back.at[g * 16 + ep], m5_s.at[g], m5_r.at[g], at_ep(dst)).start()
+
+            return c
+
+        lax.fori_loop(0, count, one, 0)
+
+    for e in range(2):
+        out[e * 16:e * 16 + 10] = finish(e, 0).reshape(10, 8, D)
+    send_back(0, 10)
     far(3)
 
     for b in range(4):
         for side, dst in ((core, att_loc), (1 - core, att_snd)):
-            rows = pl.ds(pl.multiple_of((b * 2 + side) * TOK, TOK), TOK)
-            total = jnp.sum(l_s[rows], axis=1, keepdims=True)
-            dst[b] = (acc[rows] / total).astype(BF)
+            cols = pl.ds(pl.multiple_of((b * 2 + side) * TOK, TOK), TOK)
+            total = jnp.sum(l_s[:, cols], axis=0, keepdims=True)
+            dst[b] = (acc[:, cols] / total).astype(BF)
     AT = remote(att_snd, att_rcv, at_s, at_r, mate)
     AT.start()
     AT.wait_recv()
-    heads = jnp.concatenate([att_loc[...].reshape(HALF, VDIM), att_rcv[...].reshape(HALF, VDIM)], 1)
+    heads = jnp.concatenate([jnp.concatenate([att_loc[b], att_rcv[b]], 0) for b in range(4)], 1)
     for q in range(4):
         cols = slice(q * 512, q * 512 + 512)
         w2 = jnp.concatenate([ow[0, :, cols], ow[1, :, cols]], 0)
-        pm[:, :, :, cols] = dot(heads, w2).astype(BF).reshape(4, 2, 64, 512)
+        total = lax.dot_general(heads, w2, tn, preferred_element_type=F32)
+        pm[:, :, :, cols] = total.astype(BF).reshape(4, 2, 64, 512)
     for c in TC:
         c.start()
     for k in (0, 2, 1, 3):
@@ -441,27 +495,22 @@
 
     final = []
     for e in range(2):
-        RC[1 - e].wait_recv()
-        RB[e * 2].wait_recv()
-        RB[e * 2 + 1].wait_recv()
-        whole = pp[y, e].astype(F32) + rb[e].astype(F32) + rc[1 - e].astype(F32)
-        tight = whole.astype(BF)
-        final.append(tight[128:160])
-        out[e * 16:e * 16 + 16] = tight[0:128].reshape(16, 8, D)
+        tight = finish(e, 1)
+        final.append(tight[48:80])
+        out[e * 16 + 10:e * 16 + 16] = tight[0:48].reshape(6, 8, D)
+    send_back(10, 6)
     compact = jnp.concatenate(final, 0)
     for n in range(4):
         cols = slice(n * 512, n * 512 + 512)
         wide = lax.dot_general(squeeze, compact[:, cols], tn, preferred_element_type=F32)
         outb[:, :, cols] = wide.reshape(16, 4, 512).astype(BF)
 
-    def m5(k, c):
+    def last_rows(k, c):
         dst = (ep + k) % 16
-        for g in range(2):
-            remote(out.at[g * 16 + dst], back.at[g * 16 + ep], m5_s.at[g], m5_r.at[g], at_ep(dst)).start()
         remote(outb.at[dst], backb.at[ep], m5_s.at[2], m5_r.at[2], at_ep(dst)).start()
         return c
 
-    lax.fori_loop(1, 16, m5, 0)
+    lax.fori_loop(1, 16, last_rows, 0)
     for g in range(2):
         back[g * 16 + ep] = out[g * 16 + ep]
     backb[ep] = outb[ep]
@@ -526,7 +575,7 @@
         out_specs=(vm, vm),
         scratch_shapes=[
             VM((8, TOK, LAT), BF), VM((2, 16, KVR, 128), BF), VM((GROUP, 256), BF), VM((GROUP, 256), BF),
-            VM((GROUP, 128), F32), VM((GROUP, 128), F32), VM((GROUP, 128), F32),
+            VM((8, GROUP), F32), VM((8, GROUP), F32), VM((VDIM, GROUP), F32),
             VM((4, TOK, 128), BF), VM((4, TOK, 128), BF), VM((4, TOK, 128), BF),
             VM((2, 128, D), BF), VM((2, 2, D, HID), BF), VM((2, 2, D, HID), BF), VM((2, 2, HID, D), BF),
             VM((32, 8, D), BF), VM((16, 4, D), BF), VM((4, 2, 20, 8, D), BF), VM((16, 4, D), BF), VM((32, 8, D), BF),

time: 154 us -> 138 us (0.90)
  the two profiles are of different devices: /device:TPU:102 before, /device:TPU:1 now
where the time goes in v2:
time: 138 us
  Pallas kernels  134 us (97%)
  local copies, waits for them, and re-layouts  3.76 us (3%)
    pallas_call x1, Pallas kernels, per_device(): pl.pallas_call(kernel, out_shape=(jax.ShapeDtypeStruct((TOK, D), BF), jax...  134 us
    unnamed x2, local copies, waits for them, and re-layouts  3.76 us

profile of v2, /device:TPU:1, one launch (start us, length us, event | category | flops | bytes accessed | tf_op | source)
XLA Modules:
  0.0 138.1 jit_solution(8085096426977662580)
XLA Ops:
  0.6 133.7 %shard_map.185 = (bf16[128,2048]{1,0:T(8,128)(2,1)}, bf16[128,2048]{1,0:T(8,128)(2,1)}) custom-call(bf16[128,768]{1,0:T(8,128)(2,1)} %ql_ref.1, bf16[128,512]{1,0:T(8,128)(2,1)} %kl_ref.1, bf16[64,128]{1,0:T(8,128)(2,1)} %bitcast.7, f32[768]{0:T(1024)} %qg_ref.1, f32[1,512]{1,0:T(1,128)} %bitcast.9, f32[6,128,128]{2,1,0:T(8,128)} %constant.2.clone.tab_ref, ...), custom_call_target="tpu_custom_call" | custom-call | tf_op jit(solution)/shard_map/pallas_call | solution.py:571
  134.4 1.9 %copy.22 = bf16[128,2048]{1,0:T(8,128)(2,1)} copy(bf16[128,2048]{1,0:T(8,128)(2,1)} %get-tuple-element.4) | data formatting | bytes 1048576
  136.2 1.9 %copy.23 = bf16[128,2048]{1,0:T(8,128)(2,1)} copy(bf16[128,2048]{1,0:T(8,128)(2,1)} %get-tuple-element.5) | data formatting | bytes 1048576

commit v3 on v2

--- a/solution.py
+++ b/solution.py
@@ -37,7 +37,7 @@
     omix_ref, oexp_ref,
     lat, kv, qa, qb, m_s, l_s, acc, att_loc, att_snd, att_rcv,
     ow, gw, uw, dw,
-    out, outb, xb, bb, back, backb, pp, ra, rb, rc, sb,
+    out, outb, xa, xc, bb, back, backb, pp, ra, rb, rc, sb,
     pm, ma, mb, mc, ms, sid_s, nrm,
     loc_sem, m1_s, m1_r, w_s, w_r, a1_s, a1_r, d1_s, d1_r,
     p1_s, p1_r, p2_s, p2_r, x1_s, x1_r, x2_s, x2_r,
@@ -64,7 +64,7 @@
         )
 
     barrier = pltpu.get_barrier_semaphore()
-    for dy in (1, 2, 3):
+    for dy in (1, 3):
         pl.semaphore_signal(barrier, inc=1, device_id=at_y(dy), device_id_type=MESH)
     pl.semaphore_signal(barrier, inc=1, device_id=mate, device_id_type=MESH)
 
@@ -148,24 +148,38 @@
     )
     wr = lax.dot_general(wp_ref[...], turn, tn, preferred_element_type=F32).astype(BF)
 
-    pl.semaphore_wait(barrier, 19)
-
-    def m1(k, c):
-        dst = (ep + k) % 16
-        for e in range(2):
-            remote(out.at[e * 16 + dst], xb.at[y, e, ep], m1_s.at[e], m1_r.at[e], at_ep(dst)).start()
-        remote(outb.at[dst], bb.at[ep], m1_s.at[2], m1_r.at[2], at_ep(dst)).start()
-        return c
-
-    lax.fori_loop(1, 16, m1, 0)
-    for e in range(2):
-        xb[y, e, ep] = out[e * 16 + ep]
-    bb[ep] = outb[ep]
-
-    a1 = [remote(lat.at[tp], lat.at[tp], a1_s.at[dy - 1], a1_r.at[dy - 1], at_y(dy)) for dy in (1, 2, 3)]
-    for c in (a1[0], a1[2], a1[1]):
+    pl.semaphore_wait(barrier, 18)
+
+    signs = (1, -1)
+
+    def m1(e):
+        def one(k, c):
+            dst = (ep + k) % 16
+            if e < 2:
+                remote(out.at[e * 16 + dst], xa.at[y, e, ep], m1_s.at[e], m1_r.at[e], at_ep(dst)).start()
+            else:
+                remote(outb.at[dst], bb.at[ep], m1_s.at[2], m1_r.at[2], at_ep(dst)).start()
+            return c
+
+        lax.fori_loop(1, 16, one, 0)
+
+    m1(0)
+    A1, AL, AR = [], [], []
+    rowsof = (pl.ds(0, 64), pl.ds(64, 64))
+    for d in range(2):
+        first, last = lat.at[tp, rowsof[d]], lat.at[tp, rowsof[1 - d]]
+        A1.append(remote(first, first, a1_s.at[d], a1_r.at[d], at_y(signs[d])))
+        AL.append(remote(last, last, a1_s.at[2 + d], a1_r.at[2 + d], at_y(signs[d])))
+        fw = lat.at[wrap(y - signs[d]) * 2 + core, rowsof[d]]
+        AR.append(remote(fw, fw, a1_s.at[4 + d], a1_r.at[4 + d], at_y(signs[d])))
+    for c in A1 + AL:
         c.start()
-    d1 = [remote(lat.at[tp], lat.at[tp], d1_s.at[0], d1_r.at[0], mate)]
+    m1(1)
+    m1(2)
+    d1 = []
+    for dy in (0, 1, 3, 2):
+        t = wrap(y - dy) * 2 + core
+        d1.append(remote(lat.at[t], lat.at[t], d1_s.at[dy], d1_r.at[dy], mate))
     d1[0].start()
     ws = [
         remote(gw_hbm, gw.at[1], w_s.at[0], w_r.at[0], mate),
@@ -175,16 +189,36 @@
     ]
     for c in ws:
         c.start()
-    for dy in (1, 3, 2):
-        a1[dy - 1].wait_recv()
-        t = wrap(y - dy) * 2 + core
-        c = remote(lat.at[t], lat.at[t], d1_s.at[dy], d1_r.at[dy], mate)
-        c.start()
-        d1.append(c)
-    signs = (1, -1)
     for e in range(2):
-        rep = xb.at[y, e, pl.ds(0, 15)]
+        xa[y, e, ep] = out[e * 16 + ep]
+    bb[ep] = outb[ep]
+
+    XA, XC, XR, XS = [], [], [], []
+    for d in range(2):
+        dev = at_y(signs[d])
+        XA.append([remote(xa.at[y, e], xa.at[y, e], x1_s.at[d, e], x1_r.at[d, e], dev) for e in range(2)])
+        XC.append(remote(xc.at[y], xc.at[y], x1_s.at[d, 2], x1_r.at[d, 2], dev))
+        b = wrap(y - signs[d])
+        XR.append(remote(xa.at[b, d], xa.at[b, d], x2_s.at[d, 0], x2_r.at[d, 0], dev))
+        XS.append(remote(xc.at[b, d], xc.at[b, d], x2_s.at[d, 1], x2_r.at[d, 1], dev))
+
+    def rows_here(e):
+        rep = xa.at[y, e, pl.ds(0, 15)]
         remote(rep, rep, m1_s.at[e], m1_r.at[e], mate).wait()
+        for d in range(2):
+            XA[d][e].start()
+
+    for d in range(2):
+        A1[d].wait_recv()
+        AR[d].start()
+    rows_here(0)
+    for d in range(2):
+        AL[d].wait_recv()
+        d1[1 + d].start()
+    for c in AR:
+        c.wait_recv()
+    d1[3].start()
+    rows_here(1)
     rep = bb.at[pl.ds(0, 15)]
     remote(rep, rep, m1_s.at[2], m1_r.at[2], mate).wait()
     row64 = lax.broadcasted_iota(jnp.int32, (64, 64), 0)
@@ -193,20 +227,10 @@
     squeeze = jnp.where(want == col64, 1.0, 0.0).astype(BF)
     for n in range(4):
         cols = slice(n * 512, n * 512 + 512)
-        both = bb[:, :, cols].reshape(64, 512)
-        tight = dot(squeeze, both).reshape(8, 8, 512).astype(BF)
-        for e in range(2):
-            xb[y, e, 16:20, :, cols] = tight[e * 4:e * 4 + 4]
-    X1, XL, X2 = [], [], []
-    for d in range(2):
-        first, last = xb.at[y, d], xb.at[y, 1 - d]
-        X1.append(remote(first, first, x1_s.at[d], x1_r.at[d], at_y(signs[d])))
-        XL.append(remote(last, last, x1_s.at[2 + d], x1_r.at[2 + d], at_y(signs[d])))
-        fw = xb.at[wrap(y - signs[d]), d]
-        X2.append(remote(fw, fw, x2_s.at[d], x2_r.at[d], at_y(signs[d])))
-    for c in X1:
+        tight = dot(squeeze, bb[:, :, cols].reshape(64, 512))
+        xc[y, :, :, :, cols] = tight.reshape(2, 4, 8, 512).astype(BF)
+    for c in XC:
         c.start()
-
     for c in d1:
         c.wait_recv()
 
@@ -326,14 +350,12 @@
     for h in range(2):
         for d in range(2):
             P2[h, 0, d].start()
-    for c in XL:
-        c.start()
 
     def expert(ys):
         n = len(ys)
 
         def one(e, c):
-            rows = jnp.concatenate([xb[b, e].reshape(160, D) for b in ys], 0)
+            rows = jnp.concatenate([r for b in ys for r in (xa[b, e].reshape(128, D), xc[b, e].reshape(32, D))], 0)
             total = [None] * 4
             hid = []
             for w in range(2):
@@ -417,15 +439,18 @@
     for c in ws:
         c.wait_recv()
     expert([y])
+    XA[0][0].wait_recv()
+    XR[0].start()
     p1_on()
     p2_on(0)
-    for c in X1:
-        c.wait_recv()
-    for c in X2:
-        c.start()
+    XA[1][1].wait_recv()
+    XR[1].start()
     attend_all(8, lambda n: (n // 4, (1 - n // 2 % 2) * (n % 2 * 2 - 1), n // 2 % 2 * (n % 2 * 2 - 1)))
-    for c in XL:
-        c.wait_recv()
+    for d in range(2):
+        XC[d].wait_recv()
+        XS[d].start()
+    XA[0][1].wait_recv()
+    XA[1][0].wait_recv()
     expert([wrap(y + 1), wrap(y - 1)])
     for c in RC:
         c.start()
@@ -434,7 +459,7 @@
     p2_on(2)
     attend_all(2, lambda n: (n, 2, 0))
     near(1)
-    for c in X2:
+    for c in XR + XS:
         c.wait_recv()
     expert([wrap(y + 2)])
     for k in (0, 2, 1, 3):
@@ -543,7 +568,7 @@
         whole = pm[y, e].astype(F32) + mb[e].astype(F32) + mc[1 - e].astype(F32)
         omix_ref[e * 64:e * 64 + 64] = whole.astype(BF)
 
-    for c in a1 + d1 + ws + X1 + XL + X2 + RC + RA + RB + TC + TA + TB + [AT]:
+    for c in A1 + AL + AR + d1 + ws + XA[0] + XA[1] + XC + XR + XS + RC + RA + RB + TC + TA + TB + [AT]:
         c.wait_send()
     for group in (P1, P1F, P2, P2F):
         for c in group.values():
@@ -578,13 +603,13 @@
             VM((8, GROUP), F32), VM((8, GROUP), F32), VM((VDIM, GROUP), F32),
             VM((4, TOK, 128), BF), VM((4, TOK, 128), BF), VM((4, TOK, 128), BF),
             VM((2, 128, D), BF), VM((2, 2, D, HID), BF), VM((2, 2, D, HID), BF), VM((2, 2, HID, D), BF),
-            VM((32, 8, D), BF), VM((16, 4, D), BF), VM((4, 2, 20, 8, D), BF), VM((16, 4, D), BF), VM((32, 8, D), BF),
+            VM((32, 8, D), BF), VM((16, 4, D), BF), VM((4, 2, 16, 8, D), BF), VM((4, 2, 4, 8, D), BF), VM((16, 4, D), BF), VM((32, 8, D), BF),
             VM((16, 4, D), BF),
             VM((4, 2, 160, D), BF), VM((2, 160, D), BF), VM((2, 160, D), BF), VM((2, 160, D), BF), VM((2, 160, D), BF),
             VM((4, 2, 64, D), BF), VM((2, 64, D), BF), VM((2, 64, D), BF), VM((2, 64, D), BF), VM((2, 64, D), BF),
             VM((2, TOK, 128), F32), VM((TOK, D), BF),
-            dma((4,)), dma((3,)), dma((3,)), dma((4,)), dma((4,)), dma((3,)), dma((3,)), dma((4,)), dma((4,)),
-            dma((2, 4)), dma((2, 4)), dma((2, 4, 4)), dma((2, 4, 4)), dma((4,)), dma((4,)), dma((2,)), dma((2,)),
+            dma((4,)), dma((3,)), dma((3,)), dma((4,)), dma((4,)), dma((6,)), dma((6,)), dma((4,)), dma((4,)),
+            dma((2, 4)), dma((2, 4)), dma((2, 4, 4)), dma((2, 4, 4)), dma((2, 3)), dma((2, 3)), dma((2, 2)), dma((2, 2)),
             dma((10,)), dma((10,)), dma((10,)), dma((10,)), dma, dma, dma((3,)), dma((3,)),
         ],
         compiler_params=pltpu.CompilerParams(

time: 138 us -> 132 us (0.957)
  Pallas kernels: 134 us -> 128 us
    pallas_call x1, Pallas kernels: 134 us -> 128 us  [per_device(): pl.pallas_call(kernel, out_shape=(jax.ShapeDtypeStruct((TOK, D), BF), jax...]
where the time goes in v3:
time: 132 us
  Pallas kernels  128 us (97%)
  local copies, waits for them, and re-layouts  3.76 us (3%)
    pallas_call x1, Pallas kernels, per_device(): pl.pallas_call(kernel, out_shape=(jax.ShapeDtypeStruct((TOK, D), BF), jax...  128 us
    unnamed x2, local copies, waits for them, and re-layouts  3.76 us

profile of v3, /device:TPU:1, one launch (start us, length us, event | category | flops | bytes accessed | tf_op | source)
XLA Modules:
  0.0 132.0 jit_solution(14832489360477115370)
XLA Ops:
  0.6 127.6 %shard_map.185 = (bf16[128,2048]{1,0:T(8,128)(2,1)}, bf16[128,2048]{1,0:T(8,128)(2,1)}) custom-call(bf16[128,768]{1,0:T(8,128)(2,1)} %ql_ref.1, bf16[128,512]{1,0:T(8,128)(2,1)} %kl_ref.1, bf16[64,128]{1,0:T(8,128)(2,1)} %bitcast.7, f32[768]{0:T(1024)} %qg_ref.1, f32[1,512]{1,0:T(1,128)} %bitcast.9, f32[6,128,128]{2,1,0:T(8,128)} %constant.2.clone.tab_ref, ...), custom_call_target="tpu_custom_call" | custom-call | tf_op jit(solution)/shard_map/pallas_call | solution.py:596
  128.2 1.9 %copy.22 = bf16[128,2048]{1,0:T(8,128)(2,1)} copy(bf16[128,2048]{1,0:T(8,128)(2,1)} %get-tuple-element.4) | data formatting | bytes 1048576
  130.1 1.9 %copy.23 = bf16[128,2048]{1,0:T(8,128)(2,1)} copy(bf16[128,2048]{1,0:T(8,128)(2,1)} %get-tuple-element.5) | data formatting | bytes 1048576

commit v4 on v3

--- a/solution.py
+++ b/solution.py
@@ -36,12 +36,12 @@
     xin_ref, mg_ref, routes_ref, rw_ref, ow_hbm, gw_hbm, uw_hbm, dw_hbm,
     omix_ref, oexp_ref,
     lat, kv, qa, qb, m_s, l_s, acc, att_loc, att_snd, att_rcv,
-    ow, gw, uw, dw,
+    wall, hl, hr, gw, uw, dw,
     out, outb, xa, xc, bb, back, backb, pp, ra, rb, rc, sb,
-    pm, ma, mb, mc, ms, sid_s, nrm,
+    sid_s, nrm,
     loc_sem, m1_s, m1_r, w_s, w_r, a1_s, a1_r, d1_s, d1_r,
     p1_s, p1_r, p2_s, p2_r, x1_s, x1_r, x2_s, x2_r,
-    r_s, r_r, t_s, t_r, at_s, at_r, m5_s, m5_r,
+    r_s, r_r, o1_s, o1_r, o2_s, o2_r, o4_s, o4_r, o3_s, o3_r, h_s, h_r, at_s, at_r, m5_s, m5_r,
 ):
     ep = lax.axis_index("ep")
     tp = lax.axis_index("tp")
@@ -64,7 +64,7 @@
         )
 
     barrier = pltpu.get_barrier_semaphore()
-    for dy in (1, 3):
+    for dy in (1, 2, 3):
         pl.semaphore_signal(barrier, inc=1, device_id=at_y(dy), device_id_type=MESH)
     pl.semaphore_signal(barrier, inc=1, device_id=mate, device_id_type=MESH)
 
@@ -78,7 +78,7 @@
         pltpu.make_async_copy(gw_hbm, gw.at[0], loc_sem.at[0]),
         pltpu.make_async_copy(uw_hbm, uw.at[0], loc_sem.at[1]),
         pltpu.make_async_copy(dw_hbm, dw.at[0], loc_sem.at[2]),
-        pltpu.make_async_copy(ow_hbm, ow.at[0], loc_sem.at[3]),
+        pltpu.make_async_copy(ow_hbm, wall.at[y, core], loc_sem.at[3]),
     ]
     for c in locals_:
         c.start()
@@ -148,15 +148,16 @@
     )
     wr = lax.dot_general(wp_ref[...], turn, tn, preferred_element_type=F32).astype(BF)
 
-    pl.semaphore_wait(barrier, 18)
+    pl.semaphore_wait(barrier, 19)
 
     signs = (1, -1)
+    place = ep * 13 % 16
 
     def m1(e):
         def one(k, c):
             dst = (ep + k) % 16
             if e < 2:
-                remote(out.at[e * 16 + dst], xa.at[y, e, ep], m1_s.at[e], m1_r.at[e], at_ep(dst)).start()
+                remote(out.at[e * 16 + dst], xa.at[y, e, place], m1_s.at[e], m1_r.at[e], at_ep(dst)).start()
             else:
                 remote(outb.at[dst], bb.at[ep], m1_s.at[2], m1_r.at[2], at_ep(dst)).start()
             return c
@@ -185,12 +186,20 @@
         remote(gw_hbm, gw.at[1], w_s.at[0], w_r.at[0], mate),
         remote(uw_hbm, uw.at[1], w_s.at[1], w_r.at[1], mate),
         remote(dw_hbm, dw.at[1], w_s.at[2], w_r.at[2], mate),
-        remote(ow_hbm, ow.at[1], w_s.at[3], w_r.at[3], mate),
+        remote(ow_hbm, wall.at[y, core], w_s.at[3], w_r.at[3], mate),
     ]
     for c in ws:
         c.start()
+    OP, WD = [], []
+    for dy in range(1, 4):
+        OP.append(remote(ow_hbm.at[ep], wall.at[y, core, ep], o1_s.at[dy - 1], o1_r.at[dy - 1], at_y(dy)))
+        b = wall.at[wrap(y - dy), core]
+        WD.append(remote(b, b, o3_s.at[dy - 1], o3_r.at[dy - 1], mate))
+    for c in OP:
+        c.start()
+
     for e in range(2):
-        xa[y, e, ep] = out[e * 16 + ep]
+        xa[y, e, place] = out[e * 16 + ep]
     bb[ep] = outb[ep]
 
     XA, XC, XR, XS = [], [], [], []
@@ -355,7 +364,7 @@
         n = len(ys)
 
         def one(e, c):
-            rows = jnp.concatenate([r for b in ys for r in (xa[b, e].reshape(128, D), xc[b, e].reshape(32, D))], 0)
+            rows = jnp.concatenate([r for b in ys for r in (xc[b, e].reshape(32, D), xa[b, e].reshape(128, D))], 0)
             total = [None] * 4
             hid = []
             for w in range(2):
@@ -373,32 +382,53 @@
 
         lax.fori_loop(0, 2, one, 0)
 
-    def ring(part, a_, b_, c_, s_, ssem, rsem):
-        n = part.shape[2] // 2
+    def ring(part, a_, b_, c_, s_, ssem, rsem, cuts):
         C, A, B = [], [], []
+        m = 0
         for d in range(2):
             dev = at_y(signs[d])
-            near = wrap(y + signs[d])
-            far = wrap(y + 2)
-            C.append(remote(part.at[near, 1 - d], c_.at[d], ssem.at[d], rsem.at[d], dev))
-            for k in range(2):
-                q = pl.ds(k * n, n)
-                m = 2 + d * 2 + k
-                A.append(remote(part.at[far, d, q], a_.at[d, q], ssem.at[m], rsem.at[m], dev))
-                m = 6 + d * 2 + k
-                B.append(remote(s_.at[d, q], b_.at[d, q], ssem.at[m], rsem.at[m], dev))
+            near_y = wrap(y + signs[d])
+            for lo, hi in cuts:
+                q = pl.ds(lo, hi - lo)
+                A.append(remote(part.at[wrap(y + 2), d, q], a_.at[d, q], ssem.at[m], rsem.at[m], dev))
+                B.append(remote(s_.at[d, q], b_.at[d, q], ssem.at[m + 1], rsem.at[m + 1], dev))
+                C.append(remote(part.at[near_y, 1 - d, q], c_.at[d, q], ssem.at[m + 2], rsem.at[m + 2], dev))
+                m += 3
         return C, A, B
 
-    def relay(part, a_, s_, A, B, k):
-        n = part.shape[2] // 2
-        q = slice(k * n, k * n + n)
+    def relay(part, a_, s_, A, B, cuts, k):
+        q = slice(*cuts[k])
         for d in range(2):
-            A[d * 2 + k].wait_recv()
+            n = d * len(cuts) + k
+            A[n].wait_recv()
             s_[d, q] = (part[wrap(y + signs[d]), d, q].astype(F32) + a_[d, q].astype(F32)).astype(BF)
-            B[d * 2 + k].start()
-
-    RC, RA, RB = ring(pp, ra, rb, rc, sb, r_s, r_r)
-    TC, TA, TB = ring(pm, ma, mb, mc, ms, t_s, t_r)
+            B[n].start()
+
+    cuts = ((0, 80), (80, 128), (128, 160))
+    RC, RA, RB = ring(pp, ra, rb, rc, sb, r_s, r_r, cuts)
+
+    halves = (pl.ds(0, D // 2), pl.ds(D // 2, D // 2))
+
+    def spread_first():
+        for c in OP:
+            c.wait_recv()
+        for h in range(2):
+            for k in (1, 3, 2):
+                for n in range(3):
+                    b = wall.at[wrap(y - 1 - n), core, ep, :, halves[h]]
+                    remote(b, b, o2_s.at[h, n], o2_r.at[h, n], at_ep(slot(h, k, 0))).start()
+
+    def spread_second():
+        for h in range(2):
+            for n in range(3):
+                rep = wall.at[wrap(y - 1 - n), core, pl.ds(0, 3), :, halves[h]]
+                remote(rep, rep, o2_s.at[h, n], o2_r.at[h, n], mate).wait()
+        for h in range(2):
+            for k in (1, 3, 2):
+                for i in range(4):
+                    for n in range(3):
+                        b = wall.at[wrap(y - 1 - n), core, slot(h, i, 0), :, halves[h]]
+                        remote(b, b, o4_s.at[h, n], o4_r.at[h, n], at_ep(slot(h, 0, k))).start()
 
     def p1_on():
         for h in range(2):
@@ -443,6 +473,7 @@
     XR[0].start()
     p1_on()
     p2_on(0)
+    spread_first()
     XA[1][1].wait_recv()
     XR[1].start()
     attend_all(8, lambda n: (n // 4, (1 - n // 2 % 2) * (n % 2 * 2 - 1), n // 2 % 2 * (n % 2 * 2 - 1)))
@@ -452,8 +483,11 @@
     XA[0][1].wait_recv()
     XA[1][0].wait_recv()
     expert([wrap(y + 1), wrap(y - 1)])
-    for c in RC:
-        c.start()
+    def straight(k):
+        for d in range(2):
+            RC[d * 3 + k].start()
+
+    straight(0)
     p1f_on()
     p2_on(1)
     p2_on(2)
@@ -462,41 +496,21 @@
     for c in XR + XS:
         c.wait_recv()
     expert([wrap(y + 2)])
-    for k in (0, 2, 1, 3):
+    for k in (0, 3, 1, 4, 2, 5):
         RA[k].start()
     near(2)
     p2_on(3)
+    spread_second()
     near(3, 0)
-    relay(pp, ra, sb, RA, RB, 0)
+    relay(pp, ra, sb, RA, RB, cuts, 0)
+    straight(1)
     near(3, 1)
+    relay(pp, ra, sb, RA, RB, cuts, 1)
+    straight(2)
     far(0)
-    relay(pp, ra, sb, RA, RB, 1)
+    relay(pp, ra, sb, RA, RB, cuts, 2)
     far(1)
     far(2)
-
-    def finish(e, k):
-        if k == 0:
-            RC[1 - e].wait_recv()
-        RB[e * 2 + k].wait_recv()
-        q = slice(k * 80, k * 80 + 80)
-        return (pp[y, e, q].astype(F32) + rb[e, q].astype(F32) + rc[1 - e, q].astype(F32)).astype(BF)
-
-    def send_back(first, count):
-        def one(k, c):
-            dst = first + (ep + k) % count
-
-            @pl.when(dst != ep)
-            def _():
-                for g in range(2):
-                    remote(out.at[g * 16 + dst], back.at[g * 16 + ep], m5_s.at[g], m5_r.at[g], at_ep(dst)).start()
-
-            return c
-
-        lax.fori_loop(0, count, one, 0)
-
-    for e in range(2):
-        out[e * 16:e * 16 + 10] = finish(e, 0).reshape(10, 8, D)
-    send_back(0, 10)
     far(3)
 
     for b in range(4):
@@ -507,24 +521,42 @@
     AT = remote(att_snd, att_rcv, at_s, at_r, mate)
     AT.start()
     AT.wait_recv()
-    heads = jnp.concatenate([jnp.concatenate([att_loc[b], att_rcv[b]], 0) for b in range(4)], 1)
-    for q in range(4):
-        cols = slice(q * 512, q * 512 + 512)
-        w2 = jnp.concatenate([ow[0, :, cols], ow[1, :, cols]], 0)
-        total = lax.dot_general(heads, w2, tn, preferred_element_type=F32)
-        pm[:, :, :, cols] = total.astype(BF).reshape(4, 2, 64, 512)
-    for c in TC:
+    HD = []
+    for b in (1, 3, 2):
+        to = wrap(y + b)
+        HD.append(remote(att_loc.at[to], hl.at[y], h_s.at[0, b - 1], h_r.at[0, b - 1], at_y(b)))
+        HD.append(remote(att_rcv.at[to], hr.at[y], h_s.at[1, b - 1], h_r.at[1, b - 1], at_y(b)))
+    for c in HD:
         c.start()
-    for k in (0, 2, 1, 3):
-        TA[k].start()
-
-    final = []
-    for e in range(2):
-        tight = finish(e, 1)
-        final.append(tight[48:80])
-        out[e * 16 + 10:e * 16 + 16] = tight[0:48].reshape(6, 8, D)
-    send_back(10, 6)
-    compact = jnp.concatenate(final, 0)
+    hl[y] = att_loc[y]
+    hr[y] = att_rcv[y]
+    def finish(k):
+        q = slice(*cuts[k])
+        tight = []
+        for e in range(2):
+            RB[e * 3 + k].wait_recv()
+            RC[(1 - e) * 3 + k].wait_recv()
+            tight.append((pp[y, e, q].astype(F32) + rb[e, q].astype(F32) + rc[1 - e, q].astype(F32)).astype(BF))
+        first, count = ((0, 6), (6, 6), (12, 4))[k]
+        for e in range(2):
+            rows = tight[e][32:80] if k == 0 else tight[e]
+            out[e * 16 + first:e * 16 + first + count] = rows.reshape(count, 8, D)
+
+        def one(n, c):
+            g = first + (n + ep) % count
+            dst = g * 5 % 16
+
+            @pl.when(dst != ep)
+            def _():
+                for e in range(2):
+                    remote(out.at[e * 16 + g], back.at[e * 16 + ep], m5_s.at[e], m5_r.at[e], at_ep(dst)).start()
+
+            return c
+
+        lax.fori_loop(0, count, one, 0)
+        return tight
+
+    compact = jnp.concatenate([t[0:32] for t in finish(0)], 0)
     for n in range(4):
         cols = slice(n * 512, n * 512 + 512)
         wide = lax.dot_general(squeeze, compact[:, cols], tn, preferred_element_type=F32)
@@ -536,12 +568,24 @@
         return c
 
     lax.fori_loop(1, 16, last_rows, 0)
+    finish(1)
+    for n in range(3):
+        for h in range(2):
+            rep = wall.at[wrap(y - 1 - n), core, pl.ds(0, 12), :, halves[h]]
+            remote(rep, rep, o4_s.at[h, n], o4_r.at[h, n], mate).wait()
+        WD[n].start()
+    finish(2)
     for g in range(2):
-        back[g * 16 + ep] = out[g * 16 + ep]
+        back[g * 16 + ep] = out[g * 16 + place]
     backb[ep] = outb[ep]
 
-    relay(pm, ma, ms, TA, TB, 0)
-    relay(pm, ma, ms, TA, TB, 1)
+    for c in HD + WD:
+        c.wait_recv()
+    heads = jnp.concatenate([h for b in range(4) for h in (hl[b], hr[b])], 0)
+    for q in range(4):
+        cols = slice(q * 512, q * 512 + 512)
+        w = jnp.concatenate([wall[b, k, :, :, cols].reshape(128, 512) for b in range(4) for k in (core, 1 - core)], 0)
+        omix_ref[:, cols] = lax.dot_general(heads, w, tn, preferred_element_type=F32).astype(BF)
 
     for g in range(2):
         rep = back.at[pl.ds(g * 16, 15)]
@@ -561,14 +605,7 @@
         got = [dot(pick[0], rows) + dot(pick[1], more) for pick in picks]
         oexp_ref[:, cols] = (w0 * got[0] + w1 * got[1]).astype(BF)
 
-    for e in range(2):
-        TC[1 - e].wait_recv()
-        TB[e * 2].wait_recv()
-        TB[e * 2 + 1].wait_recv()
-        whole = pm[y, e].astype(F32) + mb[e].astype(F32) + mc[1 - e].astype(F32)
-        omix_ref[e * 64:e * 64 + 64] = whole.astype(BF)
-
-    for c in A1 + AL + AR + d1 + ws + XA[0] + XA[1] + XC + XR + XS + RC + RA + RB + TC + TA + TB + [AT]:
+    for c in A1 + AL + AR + d1 + ws + XA[0] + XA[1] + XC + XR + XS + RC + RA + RB + OP + WD + HD + [AT]:
         c.wait_send()
     for group in (P1, P1F, P2, P2F):
         for c in group.values():
@@ -602,15 +639,14 @@
             VM((8, TOK, LAT), BF), VM((2, 16, KVR, 128), BF), VM((GROUP, 256), BF), VM((GROUP, 256), BF),
             VM((8, GROUP), F32), VM((8, GROUP), F32), VM((VDIM, GROUP), F32),
             VM((4, TOK, 128), BF), VM((4, TOK, 128), BF), VM((4, TOK, 128), BF),
-            VM((2, 128, D), BF), VM((2, 2, D, HID), BF), VM((2, 2, D, HID), BF), VM((2, 2, HID, D), BF),
+            VM((4, 2, 16, 8, D), BF), VM((4, 128, TOK), BF), VM((4, 128, TOK), BF), VM((2, 2, D, HID), BF), VM((2, 2, D, HID), BF), VM((2, 2, HID, D), BF),
             VM((32, 8, D), BF), VM((16, 4, D), BF), VM((4, 2, 16, 8, D), BF), VM((4, 2, 4, 8, D), BF), VM((16, 4, D), BF), VM((32, 8, D), BF),
             VM((16, 4, D), BF),
             VM((4, 2, 160, D), BF), VM((2, 160, D), BF), VM((2, 160, D), BF), VM((2, 160, D), BF), VM((2, 160, D), BF),
-            VM((4, 2, 64, D), BF), VM((2, 64, D), BF), VM((2, 64, D), BF), VM((2, 64, D), BF), VM((2, 64, D), BF),
             VM((2, TOK, 128), F32), VM((TOK, D), BF),
             dma((4,)), dma((3,)), dma((3,)), dma((4,)), dma((4,)), dma((6,)), dma((6,)), dma((4,)), dma((4,)),
             dma((2, 4)), dma((2, 4)), dma((2, 4, 4)), dma((2, 4, 4)), dma((2, 3)), dma((2, 3)), dma((2, 2)), dma((2, 2)),
-            dma((10,)), dma((10,)), dma((10,)), dma((10,)), dma, dma, dma((3,)), dma((3,)),
+            dma((18,)), dma((18,)), dma((3,)), dma((3,)), dma((2, 3)), dma((2, 3)), dma((2, 3)), dma((2, 3)), dma((3,)), dma((3,)), dma((2, 3)), dma((2, 3)), dma, dma, dma((3,)), dma((3,)),
         ],
         compiler_params=pltpu.CompilerParams(
             collective_id=0, has_side_effects=True, vmem_limit_bytes=66_000_000
@@ -618,7 +654,7 @@
     )(
         query_latent, kv_latent, rope_key.T, query_gain, kv_gain.reshape(1, -1), jnp.asarray(tables()),
         query_nope_w, query_rope_w.T, key_up_w, value_up_w, expert_in, moe_gain.reshape(1, -1), routes.T, route_weight.T,
-        output_w, gate_w, up_w, down_w,
+        output_w.reshape(16, 8, D), gate_w, up_w, down_w,
     )
 
 

time: 132 us -> 129 us (0.977)
  Pallas kernels: 128 us -> 124 us
    pallas_call x1, Pallas kernels: 128 us -> 124 us  [per_device(): pl.pallas_call(kernel, out_shape=(jax.ShapeDtypeStruct((TOK, D), BF), jax...]
where the time goes in v4:
time: 129 us; the launch traced here: 128 us
  Pallas kernels  124 us (96%)
  local copies, waits for them, and re-layouts  3.76 us (3%)
    pallas_call x1, Pallas kernels, per_device(): pl.pallas_call(kernel, out_shape=(jax.ShapeDtypeStruct((TOK, D), BF), jax...  124 us
    unnamed x2, local copies, waits for them, and re-layouts  3.76 us

profile of v4, /device:TPU:1, one launch (start us, length us, event | category | flops | bytes accessed | tf_op | source)
XLA Modules:
  0.0 128.5 jit_solution(1691903748159148778)
XLA Ops:
  0.6 124.0 %shard_map.185 = (bf16[128,2048]{1,0:T(8,128)(2,1)}, bf16[128,2048]{1,0:T(8,128)(2,1)}) custom-call(bf16[128,768]{1,0:T(8,128)(2,1)} %ql_ref.1, bf16[128,512]{1,0:T(8,128)(2,1)} %kl_ref.1, bf16[64,128]{1,0:T(8,128)(2,1)} %bitcast.9, f32[768]{0:T(1024)} %qg_ref.1, f32[1,512]{1,0:T(1,128)} %bitcast.11, f32[6,128,128]{2,1,0:T(8,128)} %constant.2.clone.tab_ref, ...), custom_call_target="tpu_custom_call" | custom-call | tf_op jit(solution)/shard_map/pallas_call | solution.py:633
  124.7 1.9 %copy.22 = bf16[128,2048]{1,0:T(8,128)(2,1)} copy(bf16[128,2048]{1,0:T(8,128)(2,1)} %get-tuple-element.4) | data formatting | bytes 1048576
  126.6 1.9 %copy.23 = bf16[128,2048]{1,0:T(8,128)(2,1)} copy(bf16[128,2048]{1,0:T(8,128)(2,1)} %get-tuple-element.5) | data formatting | bytes 1048576

commit v5 on v4

--- a/solution.py
+++ b/solution.py
@@ -34,7 +34,7 @@
 def kernel(
     ql_ref, kl_ref, rk_ref, qg_ref, kg_ref, tab_ref, wq_ref, wp_ref, wk_ref, wv_ref,
     xin_ref, mg_ref, routes_ref, rw_ref, ow_hbm, gw_hbm, uw_hbm, dw_hbm,
-    omix_ref, oexp_ref,
+    both_ref,
     lat, kv, qa, qb, m_s, l_s, acc, att_loc, att_snd, att_rcv,
     wall, hl, hr, gw, uw, dw,
     out, outb, xa, xc, bb, back, backb, pp, ra, rb, rc, sb,
@@ -585,7 +585,7 @@
     for q in range(4):
         cols = slice(q * 512, q * 512 + 512)
         w = jnp.concatenate([wall[b, k, :, :, cols].reshape(128, 512) for b in range(4) for k in (core, 1 - core)], 0)
-        omix_ref[:, cols] = lax.dot_general(heads, w, tn, preferred_element_type=F32).astype(BF)
+        both_ref[0, :, cols] = lax.dot_general(heads, w, tn, preferred_element_type=F32).astype(BF)
 
     for g in range(2):
         rep = back.at[pl.ds(g * 16, 15)]
@@ -603,7 +603,7 @@
         rows = back[:, :, cols].reshape(256, 512)
         more = backb[:, :, cols].reshape(64, 512)
         got = [dot(pick[0], rows) + dot(pick[1], more) for pick in picks]
-        oexp_ref[:, cols] = (w0 * got[0] + w1 * got[1]).astype(BF)
+        both_ref[1, :, cols] = (w0 * got[0] + w1 * got[1]).astype(BF)
 
     for c in A1 + AL + AR + d1 + ws + XA[0] + XA[1] + XC + XR + XS + RC + RA + RB + OP + WD + HD + [AT]:
         c.wait_send()
@@ -630,11 +630,11 @@
     dma = pltpu.SemaphoreType.DMA
     vm = pl.BlockSpec(memory_space=VM)
     hbm = pl.BlockSpec(memory_space=pl.ANY)
-    return pl.pallas_call(
+    both = pl.pallas_call(
         kernel,
-        out_shape=(jax.ShapeDtypeStruct((TOK, D), BF), jax.ShapeDtypeStruct((TOK, D), BF)),
+        out_shape=jax.ShapeDtypeStruct((2, TOK, D), BF),
         in_specs=[vm] * 14 + [hbm] * 4,
-        out_specs=(vm, vm),
+        out_specs=vm,
         scratch_shapes=[
             VM((8, TOK, LAT), BF), VM((2, 16, KVR, 128), BF), VM((GROUP, 256), BF), VM((GROUP, 256), BF),
             VM((8, GROUP), F32), VM((8, GROUP), F32), VM((VDIM, GROUP), F32),
@@ -656,6 +656,7 @@
         query_nope_w, query_rope_w.T, key_up_w, value_up_w, expert_in, moe_gain.reshape(1, -1), routes.T, route_weight.T,
         output_w.reshape(16, 8, D), gate_w, up_w, down_w,
     )
+    return both[0], both[1]
 
 
 def solution(mesh):

time: 129 us -> 127 us (0.984)
  local copies, waits for them, and re-layouts: 3.76 us -> 2.28 us
    unnamed x2 -> x0, local copies, waits for them, and re-layouts: 3.76 us -> none
    squeeze x0 -> x1, local copies, waits for them, and re-layouts: none -> 2.28 us  [per_device(): return (both[0], both[1])]
where the time goes in v5:
time: 127 us
  Pallas kernels  124 us (98%)
  local copies, waits for them, and re-layouts  2.28 us (2%)
    pallas_call x1, Pallas kernels, per_device(): pl.pallas_call(kernel, out_shape=jax.ShapeDtypeStruct((2, TOK, D), BF), i...  124 us

profile of v5, /device:TPU:1, one launch (start us, length us, event | category | flops | bytes accessed | tf_op | source)
XLA Modules:
  0.0 127.0 jit_solution(4616342888336879653)
XLA Ops:
  0.6 124.0 %shard_map.185 = bf16[2,128,2048]{2,1,0:T(8,128)(2,1)} custom-call(bf16[128,768]{1,0:T(8,128)(2,1)} %ql_ref.1, bf16[128,512]{1,0:T(8,128)(2,1)} %kl_ref.1, bf16[64,128]{1,0:T(8,128)(2,1)} %bitcast.13, f32[768]{0:T(1024)} %qg_ref.1, f32[1,512]{1,0:T(1,128)} %bitcast.15, f32[6,128,128]{2,1,0:T(8,128)} %constant.2.clone.tab_ref, bf16[768,128]{1,0:T(8,128)(2,1)} %wq_ref.1, ...), custom_call_target="tpu_custom_call" | custom-call | tf_op jit(solution)/shard_map/pallas_call | solution.py:633
  124.7 2.3 %slice_bitcast_fusion = (bf16[128,2048]{1,0:T(8,128)(2,1)}, bf16[128,2048]{1,0:T(8,128)(2,1)}) fusion(bf16[2,128,2048]{2,1,0:T(8,128)(2,1)} %shard_map.185), kind=kLoop, calls=%fused_computation | loop fusion | bytes 2097152 | tf_op jit(solution)/shard_map/squeeze | solution.py:659
